TPU v7x, 512 devices: a whole 4x8x8 slice. The times are simulated.
512 devices in a mesh: tp: 32 (over z, x), dp: 16 (over y, core).
Axes of the slice: x: 4, y: 8, z: 8, core: 2. Of those that a mesh axis runs over, the one named last changes fastest.
Arguments:
- tokens: bfloat16 [256, 4096], P('dp', 'tp'), may hold values from -6 to 6
- norm_gain: float32 [2, 4096], replicated, may hold values from 0.1 to 1.9
- w_in: bfloat16 [2, 4096, 2048], P(None, 'dp', 'tp'), may hold values from -0.09375 to 0.09375
- w_gate: bfloat16 [2, 4096, 2048], P(None, 'dp', 'tp'), may hold values from -0.1875 to 0.1875
- decay_rate: float32 [2, 128, 64], P(None, 'tp'), may hold values from 0.05 to 2
- frequency: float32 [2, 128, 64], P(None, 'tp'), may hold values from -3 to 3
- log_step: float32 [2, 128], P(None, 'tp'), may hold values from -3 to 0
- map_re: float32 [2, 128, 16, 64], P(None, 'tp'), may hold values from -1.5 to 1.5
- map_im: float32 [2, 128, 16, 64], P(None, 'tp'), may hold values from -1.5 to 1.5
- read_re: float32 [2, 128, 16, 64], P(None, 'tp'), may hold values from -0.5 to 0.5
- read_im: float32 [2, 128, 16, 64], P(None, 'tp'), may hold values from -0.5 to 0.5
- skip_weight: float32 [2, 128, 16], P(None, 'tp'), may hold values from -4 to 4
- w_out: bfloat16 [2, 2048, 4096], P(None, 'dp', 'tp'), may hold values from -0.25 to 0.25
- state_re: float32 [2, 256, 128, 64], P(None, 'dp', 'tp'), may hold values from -6 to 6
- state_im: float32 [2, 256, 128, 64], P(None, 'dp', 'tp'), may hold values from -6 to 6
Outputs:
- hidden: bfloat16 [256, 4096], P('dp', 'tp')
- new_re: float32 [2, 256, 128, 64], P(None, 'dp', 'tp')
- new_im: float32 [2, 256, 128, 64], P(None, 'dp', 'tp')
All inputs are finite; a program needn't handle non-finite values.
Results may differ from a plain program's by a relative error of at most 0.01.
Values may be sent and summed in bfloat16 or wider, within the bound.
No kernel may reach another device: no remote copies, remote signals or barrier semaphores. Data moves between devices by JAX's collectives and lax.ppermute only.
A program may use at most 64 MiB of HBM per device.

v0:
```python
import functools

import jax
import jax.numpy as jnp
from jax import lax
from jax.experimental import pallas as pl
from jax.experimental.pallas import tpu as pltpu
from jax.sharding import PartitionSpec as P


EPSILON = 1e-06
HIGH = lax.Precision.HIGHEST
F32 = jnp.float32
BF16 = jnp.bfloat16


PARTNER = [(i, i ^ 1) for i in range(16)]
SAME_CORE = [[2 * y + c for y in range(8)] for c in range(2)]
ROUND = [(2 * y, 2 * ((y + 1) % 8)) for y in range(8)] + [(2 * y + 1, 2 * ((y - 1) % 8) + 1) for y in range(8)]


def to_partner(array):
    return lax.ppermute(array, "dp", PARTNER)


def along_y(copies):
    return lax.all_to_all(copies, "dp", split_axis=0, concat_axis=0, tiled=True, axis_index_groups=SAME_CORE)


def behind(array, *others):
    return lax.optimization_barrier((array, *others))[0]


def round_step(piece):
    return lax.ppermute(piece, "dp", ROUND)


def block_of(here, i):
    y, c = here >> 1, here & 1
    k = i // 2
    step = k if k < 5 else 4 - k
    core = c if (i % 2 == 1) == (k >= 5) else 1 - c
    return 2 * ((y + (2 * c - 1) * step) & 7) + core


def shards_of(layer, here, pieces):
    if layer == 0:
        return [(2 * (i % 8) + ((here & 1) ^ (i // 8)), pieces[i // 8], i % 8) for i in range(16)]
    ring = [(block_of(here, i), pieces[i // 2], i % 2) for i in range(10)]
    return ring + [(block_of(here, i), pieces[5], i - 10) for i in range(10, 16)]


def over_tp(copies):
    return lax.all_to_all(copies, "tp", split_axis=0, concat_axis=0, tiled=True)


def loaded(kernel, count):
    def body(*refs):
        sources, sems = refs[:count], refs[-1]
        outs, local = refs[count : -count - 1], refs[-count - 1 : -1]
        copies = [pltpu.make_async_copy(a, b, sems.at[i]) for i, (a, b) in enumerate(zip(sources, local))]
        for copy in copies:
            copy.start()
        for copy in copies:
            copy.wait()
        kernel(*local, *outs)

    return body


def send_kernel(w_in, w_gate, w_out, first, second):
    for y in range(8):
        first[y, 0:64, 0:256] = w_in[0]
        first[y, 64:128, 0:256] = w_gate[0]
        first[y, :, 256:384] = w_out[0]
    second[0:64, 0:256] = w_in[1]
    second[64:128, 0:256] = w_gate[1]
    second[:, 256:384] = w_out[1]


def copy_kernel(tokens, *rest):
    rest[-1][...] = jnp.broadcast_to(tokens[...][None], rest[-1].shape)


def prepare_kernel(gains, decay_rate, frequency, log_step, map_re, map_im, read_re, read_im, skip_weight, state_re, state_im, gain, drive, read, decay, skip, old):
    drive[...] = jnp.zeros(drive.shape, F32)
    read[...] = jnp.zeros(read.shape, F32)
    skip[...] = jnp.zeros(skip.shape, F32)
    for t in range(32):
        gain[:, t, :] = gains[:, 128 * t : 128 * t + 128]
    for l in range(2):
        lam_re = -decay_rate[l]
        lam_im = frequency[l]
        step_size = jnp.exp(log_step[l])
        magnitude = jnp.exp(lam_re * step_size)
        decay_re = magnitude * jnp.cos(lam_im * step_size)
        decay_im = magnitude * jnp.sin(lam_im * step_size)
        modulus = lam_re * lam_re + lam_im * lam_im
        hold_re = ((decay_re - 1.0) * lam_re + decay_im * lam_im) / modulus
        hold_im = (decay_im * lam_re - (decay_re - 1.0) * lam_im) / modulus
        for g in range(4):
            rows, at = slice(16 * g, 16 * g + 16), 64 * g
            h_re, h_im = hold_re[g : g + 1], hold_im[g : g + 1]
            m_re, m_im = map_re[l, g], map_im[l, g]
            drive[l, rows, at : at + 64] = h_re * m_re - h_im * m_im
            drive[l, rows, at + 256 : at + 320] = h_re * m_im + h_im * m_re
            read[l, rows, at : at + 64] = read_re[l, g]
            read[l, rows, at + 256 : at + 320] = -read_im[l, g]
            decay[l, 0:1, at : at + 64] = decay_re[g : g + 1]
            decay[l, 1:2, at : at + 64] = decay_im[g : g + 1]
            skip[l, 0:1, 16 * g : 16 * g + 16] = skip_weight[l, g : g + 1]
            old[l, 0, :, at : at + 64] = state_re[l, :, g, :]
            old[l, 1, :, at : at + 64] = state_im[l, :, g, :]


def mixer_kernel(layer, here, x, gain, drive_far, read_far, decay, skip, old, *rest):
    pieces, (mixed, fresh_out, drive, read, sems) = rest[:-5], rest[-5:]
    get_drive = pltpu.make_async_copy(drive_far.at[layer], drive, sems.at[0])
    get_read = pltpu.make_async_copy(read_far.at[layer], read, sems.at[1])
    get_drive.start()
    get_read.start()
    wide = x[...].astype(F32)
    square = jnp.sum(jnp.sum(wide * wide, axis=0), axis=1, keepdims=True)
    inv_scale = lax.rsqrt(square * (1.0 / 4096) + EPSILON)
    total = jnp.zeros((16, 128), F32)
    for block, array, at in shards_of(layer, here[0], pieces):
        t = 2 * block
        left = (x[t].astype(F32) * inv_scale * gain[layer, pl.ds(t, 1), :]).astype(BF16)
        right = (x[t + 1].astype(F32) * inv_scale * gain[layer, pl.ds(t + 1, 1), :]).astype(BF16)
        rows = jnp.concatenate([left, right], axis=1)
        total += lax.dot_general(rows, array[at, :, 0:256], (((1,), (1,)), ((), ())), preferred_element_type=F32)
    both = total.astype(BF16).astype(F32)
    get_drive.wait()
    push = jnp.dot(both, drive[...], precision=HIGH, preferred_element_type=F32)
    d_re, d_im = decay[layer, 0:1], decay[layer, 1:2]
    o_re, o_im = old[layer, 0], old[layer, 1]
    f_re = d_re * o_re - d_im * o_im + push[:, :256]
    f_im = d_re * o_im + d_im * o_re + push[:, 256:]
    fresh = jnp.concatenate([f_re, f_im], axis=1)
    fresh_out[...] = fresh
    get_read.wait()
    readout = lax.dot_general(fresh, read[...], (((1,), (1,)), ((), ())), precision=HIGH, preferred_element_type=F32)
    readout = readout + skip[layer] * both
    gate = pltpu.roll(both, 64, axis=1)
    mixer = (jax.nn.gelu(readout) * jax.nn.sigmoid(gate)).astype(BF16).astype(F32)
    packed = (mixer[:8] + pltpu.roll(mixer[8:], 64, axis=1)).astype(BF16)
    mixed[...] = jnp.broadcast_to(packed[None], mixed.shape)


def out_kernel(layer, here, mixed, before, *rest):
    count = 2 if layer == 0 else 6
    pieces, outs = rest[:count], rest[count:]
    low = lax.broadcasted_iota(jnp.int32, (8, 128), 1) < 64
    total = jnp.zeros((16, 128), F32)
    for block, array, at in shards_of(layer, here[0], pieces):
        t = 2 * block
        a = mixed[t].astype(F32)
        b = mixed[t + 1].astype(F32)
        upper = jnp.where(low, a, pltpu.roll(b, 64, axis=1))
        lower = jnp.where(low, pltpu.roll(a, 64, axis=1), b)
        rows = jnp.concatenate([upper, lower], axis=0).astype(BF16)
        total += jnp.dot(rows, array[at, :, 256:384], preferred_element_type=F32)
    hidden = (before[...].astype(F32) + total).astype(BF16)
    if layer == 0:
        outs[0][...] = hidden
        outs[1][...] = jnp.broadcast_to(hidden[None], outs[1].shape)
        return
    fresh, (out, new_re, new_im) = outs[:2], outs[2:]
    out[...] = hidden
    for l in range(2):
        for g in range(4):
            new_re[l, :, g, :] = fresh[l][:, 64 * g : 64 * g + 64]
            new_im[l, :, g, :] = fresh[l][:, 64 * g + 256 : 64 * g + 320]


VMEM = pl.BlockSpec(memory_space=pltpu.VMEM)
SMEM = pl.BlockSpec(memory_space=pltpu.SMEM)


def close(*arrays):
    return [pltpu.with_memory_space_constraint(a, pltpu.VMEM) for a in arrays]


def run(kernel, args, shapes, near=(), smem=0):
    return pl.pallas_call(
        kernel,
        in_specs=[SMEM] * smem + [VMEM] * (len(args) - smem),
        out_specs=[VMEM] * len(shapes),
        out_shape=[pltpu.VMEM(*s) if i in near else jax.ShapeDtypeStruct(*s) for i, s in enumerate(shapes)],
        compiler_params=pltpu.CompilerParams(vmem_limit_bytes=16 << 20),
    )(*args)


def run_loaded(kernel, args, shapes, near=()):
    args = [pltpu.with_memory_space_constraint(a, pltpu.HBM) for a in args]
    return pl.pallas_call(
        loaded(kernel, len(args)),
        in_specs=[pl.BlockSpec(memory_space=pltpu.HBM)] * len(args),
        out_specs=[VMEM] * len(shapes),
        out_shape=[pltpu.VMEM(*s) if i in near else jax.ShapeDtypeStruct(*s) for i, s in enumerate(shapes)],
        scratch_shapes=[pltpu.VMEM(a.shape, a.dtype) for a in args] + [pltpu.SemaphoreType.DMA((len(args),))],
        compiler_params=pltpu.CompilerParams(vmem_limit_bytes=16 << 20),
    )(*args)


def mixer_call(layer, here, x, small, pieces):
    gain, drive, read, decay, skip, old = small
    args = [here, *close(x, gain), drive, read, *close(decay, skip, old, *pieces)]
    specs = [SMEM] + [VMEM] * (len(args) - 1)
    for at in (3, 4):
        args[at] = pltpu.with_memory_space_constraint(args[at], pltpu.HBM)
        specs[at] = pl.BlockSpec(memory_space=pltpu.HBM)
    return pl.pallas_call(
        functools.partial(mixer_kernel, layer),
        in_specs=specs,
        out_specs=[VMEM] * 2,
        out_shape=[jax.ShapeDtypeStruct((32, 8, 128), BF16), pltpu.VMEM((16, 512), F32)],
        scratch_shapes=[pltpu.VMEM((128, 512), F32)] * 2 + [pltpu.SemaphoreType.DMA((2,))],
        compiler_params=pltpu.CompilerParams(vmem_limit_bytes=16 << 20),
        name="mixer_step",
    )(*args)


def copy_call(tokens, *after):
    return pl.pallas_call(
        copy_kernel,
        in_specs=[VMEM] + [pl.BlockSpec(memory_space=pl.ANY)] * len(after),
        out_specs=VMEM,
        out_shape=jax.ShapeDtypeStruct((32, 16, 128), BF16),
        compiler_params=pltpu.CompilerParams(vmem_limit_bytes=16 << 20),
        name="copy_step",
    )(tokens, *after)


def local(tokens, norm_gain, w_in, w_gate, decay_rate, frequency, log_step, map_re, map_im, read_re, read_im, skip_weight, w_out, state_re, state_im):
    here = lax.axis_index("dp").astype(jnp.int32).reshape(1)
    first, second = run_loaded(
        send_kernel,
        (w_in.transpose(0, 2, 1), w_gate.transpose(0, 2, 1), w_out),
        [((8, 128, 384), BF16), ((128, 384), BF16)],
        (1,),
    )
    small = run_loaded(
        prepare_kernel,
        (norm_gain, decay_rate, frequency, log_step[:, :, None], map_re, map_im, read_re, read_im, skip_weight, state_re, state_im),
        [((2, 32, 128), F32), ((2, 128, 512), F32), ((2, 128, 512), F32), ((2, 2, 256), F32), ((2, 1, 128), F32), ((2, 2, 16, 256), F32)],
        (0, 3, 4, 5),
    )
    w_own = along_y(first)
    pieces = [jnp.stack([second, to_partner(second)])]
    pieces.append(round_step(pieces[0]))
    w_other = to_partner(w_own)
    copies = copy_call(tokens, small[3])
    gathered = over_tp(copies)
    pieces.append(round_step(behind(pieces[1], w_own)))
    mixed, fresh0 = mixer_call(0, here, gathered, small, (w_own, w_other))
    pieces.append(round_step(behind(pieces[2], fresh0)))
    mixed = over_tp(mixed)
    shapes = [((16, 128), BF16), ((32, 16, 128), BF16)]
    hidden, copies = run(functools.partial(out_kernel, 0), (here, *close(mixed), tokens, *close(w_own, w_other)), shapes, (0,), 1)
    pieces.append(round_step(behind(pieces[3], hidden)))
    pieces.append(to_partner(behind(jnp.concatenate(pieces[1:4]), hidden)))
    mixed, fresh1 = mixer_call(1, here, over_tp(copies), small, pieces)
    shapes = [((16, 128), BF16), (state_re.shape, F32), (state_im.shape, F32)]
    args = (here, *close(over_tp(mixed), hidden, *pieces, fresh0, fresh1))
    return tuple(run(functools.partial(out_kernel, 1), args, shapes, (), 1))


def solution(mesh):
    return jax.shard_map(
        local,
        mesh=mesh,
        in_specs=(
            P("dp", "tp"),
            P(),
            P(None, "dp", "tp"),
            P(None, "dp", "tp"),
            P(None, "tp", None),
            P(None, "tp", None),
            P(None, "tp"),
            P(None, "tp", None, None),
            P(None, "tp", None, None),
            P(None, "tp", None, None),
            P(None, "tp", None, None),
            P(None, "tp", None),
            P(None, "dp", "tp"),
            P(None, "dp", "tp", None),
            P(None, "dp", "tp", None),
        ),
        out_specs=(P("dp", "tp"), P(None, "dp", "tp", None), P(None, "dp", "tp", None)),
        check_vma=False,
    )
```

profile of v0, /device:TPU:2, one launch (start us, length us, event | category | flops | bytes accessed | tf_op | source)
XLA Modules:
  0.0 124.5 jit_solution(10212061441099166832)
XLA Ops:
  0.6 1.0 shard_map.167
  1.6 30.0 %all_to_all.25.rest_0_ = bf16[8,128,384]{2,1,0:T(8,128)(2,1)S(1)} all-to-all(bf16[8,128,384]{2,1,0:T(8,128)(2,1)S(1)} %get-tuple-element.27), channel_id=1, replica_groups={{0,2,4,6,8,10,12,14},{1,3,5,7,9,11,13,15},{16,18,20,22,24,26,28,30},{17..., dimensions={0} | all-to-all | bytes 1572864 | tf_op jit(solution)/shard_map/all_to_all | solution.py:27
  31.7 1.9 %collective-permute-start = (bf16[8,128,384]{2,1,0:T(8,128)(2,1)S(1)}, bf16[8,128,384]{2,1,0:T(8,128)(2,1)S(1)}, u32[]{:S(2)}, u32[]{:S(2)}) collective-permute-start(bf16[8,128,384]{2,1,0:T(8,128)(2,1)S(1)} %all_to_all.25.rest_0_), channel_id=1, source_target_pairs={{0,1},{1,0},{2,3},{3,2},{4,5},{5,4},{6,7},{7,6},{8,9},{9,8},{10,11... | collective-permute-start | bytes 2359304 | tf_op jit(solution)/shard_map/ppermute | solution.py:23
  33.6 2.4 %collective-permute-start.1 = (bf16[128,384]{1,0:T(8,128)(2,1)S(1)}, bf16[128,384]{1,0:T(8,128)(2,1)S(1)}, u32[]{:S(2)}, u32[]{:S(2)}) collective-permute-start(bf16[128,384]{1,0:T(8,128)(2,1)S(1)} %get-tuple-element.30), channel_id=1, source_target_pairs={{0,1},{1,0},{2,3},{3,2},{4,5},{5,4},{6,7},{7,6},{8,9},{9,8},{10,11... | collective-permute-start | bytes 294920 | tf_op jit(solution)/shard_map/ppermute | solution.py:23
  36.0 0.9 collective-permute-done.1
  36.9 0.0 copy-start.3
  37.0 2.5 %collective-permute-start.2 = (bf16[2,128,384]{2,1,0:T(8,128)(2,1)S(1)}, bf16[2,128,384]{2,1,0:T(8,128)(2,1)S(1)}, u32[]{:S(2)}, u32[]{:S(2)}) collective-permute-start(bf16[2,128,384]{2,1,0:T(8,128)(2,1)S(1)} %pad_maximum_fusion.1.rest_0_), channel_id=1, source_target_pairs={{0,2},{2,4},{4,6},{6,8},{8,10},{10,12},{12,14},{14,0},{1,15},{3,1}... | collective-permute-start | bytes 589832 | tf_op jit(solution)/shard_map/ppermute | solution.py:35
  39.4 0.0 copy-done.3
  39.4 0.7 copy.18.refs_3_
  40.1 0.0 copy-start.2
  40.1 1.5 %shard_map.166 = (f32[2,32,128]{2,1,0:T(8,128)S(1)}, f32[2,128,512]{2,1,0:T(8,128)S(1)}, f32[2,128,512]{2,1,0:T(8,128)S(1)}, f32[2,2,256]{2,1,0:T(2,128)S(1)}, f...) custom-call(f32[2,4096]{1,0:T(2,128)} %refs_0_.1, f32[2,4,64]{2,1,0:T(4,128)} %refs_1_.1, f32[2,4,64]{2,1,0:T(4,128)} %refs_2_.2, ...), custom_call_target="tpu_custom_call" | custom-call | tf_op jit(solution)/shard_map/pallas_call | solution.py:196
  41.6 0.0 copy-start
  41.6 0.8 copy-done
  42.4 0.0 copy-start.1
  42.4 0.8 copy-done.1
  43.2 0.0 copy-done.2
  43.2 0.7 copy_step.1
  43.9 13.5 %all-to-all-start = ((bf16[32,16,128]{2,1,0:T(8,128)(2,1)}), bf16[32,16,128]{2,1,0:T(8,128)(2,1)S(1)}, u32[]{:S(2)}, u32[]{:S(2)}) async-start(bf16[32,16,128]{2,1,0:T(8,128)(2,1)} %copy_step.1), calls=%async_computation | async-start | bytes 262144 | tf_op jit(solution)/shard_map/all_to_all | solution.py:54
  57.3 0.0 collective-permute-done.2.rest_1_
  57.4 1.9 %collective-permute-start.3 = (bf16[2,128,384]{2,1,0:T(8,128)(2,1)S(1)}, bf16[2,128,384]{2,1,0:T(8,128)(2,1)S(1)}, u32[]{:S(2)}, u32[]{:S(2)}) collective-permute-start(bf16[2,128,384]{2,1,0:T(8,128)(2,1)S(1)} %collective-permute-done.2.rest_1_), channel_id=1, source_target_pairs={{0,2},{2,4},{4,6},{6,8},{8,10},{10,12},{12,14},{14,0},{1,15},{3,1}... | collective-permute-start | bytes 589832 | tf_op jit(solution)/shard_map/ppermute | solution.py:35
  59.3 6.9 %all-to-all-done.x = bf16[32,16,128]{2,1,0:T(8,128)(2,1)S(1)} async-done(((bf16[32,16,128]{2,1,0:T(8,128)(2,1)}), bf16[32,16,128]{2,1,0:T(8,128)(2,1)S(1)}, u32[]{:S(2)}, u32[]{:S(2)}) %all-to-all-start) | async-done | bytes 131104 | tf_op jit(solution)/shard_map/all_to_all | solution.py:54
  66.2 0.0 collective-permute-done.rest_1_
  66.2 1.9 %mixer_step.2 = (bf16[32,8,128]{2,1,0:T(8,128)(2,1)S(1)}, f32[16,512]{1,0:T(8,128)S(1)}) custom-call(s32[1]{0:T(128)} %bitcast.here, bf16[32,16,128]{2,1,0:T(8,128)(2,1)S(1)} %all-to-all-done.x, f32[2,32,128]{2,1,0:T(8,128)S(1)} %get-tuple-element.22.gain, f32[2,128,512]{2,1,0:T(8,128)} %copy-done, f32[2,128,512]{2,1,0:T(8,128)} %copy-done.1, ...), custom_call_target="tpu_custom_call" | custom-call | tf_op jit(solution)/shard_map/mixer_step/pallas_call | solution.py:213
  68.1 0.0 collective-permute-done.3.rest_2_
  68.1 2.4 %collective-permute-start.4 = (bf16[2,128,384]{2,1,0:T(8,128)(2,1)S(1)}, bf16[2,128,384]{2,1,0:T(8,128)(2,1)S(1)}, u32[]{:S(2)}, u32[]{:S(2)}) collective-permute-start(bf16[2,128,384]{2,1,0:T(8,128)(2,1)S(1)} %collective-permute-done.3.rest_2_), channel_id=1, source_target_pairs={{0,2},{2,4},{4,6},{6,8},{8,10},{10,12},{12,14},{14,0},{1,15},{3,1}... | collective-permute-start | bytes 589832 | tf_op jit(solution)/shard_map/ppermute | solution.py:35
  70.6 15.8 %all_to_all.26.mixed = bf16[32,8,128]{2,1,0:T(8,128)(2,1)S(1)} all-to-all(bf16[32,8,128]{2,1,0:T(8,128)(2,1)S(1)} %get-tuple-element.28), channel_id=1, replica_groups=mesh['tp'=32,'dp'=16] {'tp'}, dimensions={0} | all-to-all | bytes 131072 | tf_op jit(solution)/shard_map/all_to_all | solution.py:54
  86.3 1.0 shard_map.168
  87.3 0.0 collective-permute-done.4.rest_3_
  87.3 0.1 pad_maximum_fusion
  87.4 1.9 %collective-permute-start.6 = (bf16[6,128,384]{2,1,0:T(8,128)(2,1)S(1)}, bf16[6,128,384]{2,1,0:T(8,128)(2,1)S(1)}, u32[]{:S(2)}, u32[]{:S(2)}) collective-permute-start(bf16[6,128,384]{2,1,0:T(8,128)(2,1)S(1)} %pad_maximum_fusion), channel_id=1, source_target_pairs={{0,1},{1,0},{2,3},{3,2},{4,5},{5,4},{6,7},{7,6},{8,9},{9,8},{10,11... | collective-permute-start | bytes 1769480 | tf_op jit(solution)/shard_map/ppermute | solution.py:23
  89.3 5.0 %all-to-all-start.3 = ((bf16[32,16,128]{2,1,0:T(8,128)(2,1)}), bf16[32,16,128]{2,1,0:T(8,128)(2,1)S(1)}, u32[]{:S(2)}, u32[]{:S(2)}) async-start(bf16[32,16,128]{2,1,0:T(8,128)(2,1)} %get-tuple-element.29), calls=%async_computation.3 | async-start | bytes 262144 | tf_op jit(solution)/shard_map/all_to_all | solution.py:54
  94.4 1.9 %collective-permute-start.5 = (bf16[2,128,384]{2,1,0:T(8,128)(2,1)S(1)}, bf16[2,128,384]{2,1,0:T(8,128)(2,1)S(1)}, u32[]{:S(2)}, u32[]{:S(2)}) collective-permute-start(bf16[2,128,384]{2,1,0:T(8,128)(2,1)S(1)} %collective-permute-done.4.rest_3_), channel_id=1, source_target_pairs={{0,2},{2,4},{4,6},{6,8},{8,10},{10,12},{12,14},{14,0},{1,15},{3,1}... | collective-permute-start | bytes 589832 | tf_op jit(solution)/shard_map/ppermute | solution.py:35
  96.3 7.7 %all-to-all-done.3.x = bf16[32,16,128]{2,1,0:T(8,128)(2,1)S(1)} async-done(((bf16[32,16,128]{2,1,0:T(8,128)(2,1)}), bf16[32,16,128]{2,1,0:T(8,128)(2,1)S(1)}, u32[]{:S(2)}, u32[]{:S(2)}) %all-to-all-start.3) | async-done | bytes 131104 | tf_op jit(solution)/shard_map/all_to_all | solution.py:54
  104.0 0.0 collective-permute-done.5.rest_4_
  104.0 0.0 collective-permute-done.6.rest_5_
  104.0 2.0 %mixer_step.3 = (bf16[32,8,128]{2,1,0:T(8,128)(2,1)S(1)}, f32[16,512]{1,0:T(8,128)S(1)}) custom-call(s32[1]{0:T(128)} %bitcast.here, bf16[32,16,128]{2,1,0:T(8,128)(2,1)S(1)} %all-to-all-done.3.x, f32[2,32,128]{2,1,0:T(8,128)S(1)} %get-tuple-element.22.gain, f32[2,128,512]{2,1,0:T(8,128)} %copy-done, f32[2,128,512]{2,1,0:T(8,128)} %copy-done.1, ...), custom_call_target="tpu_custom_call" | custom-call | tf_op jit(solution)/shard_map/mixer_step/pallas_call | solution.py:213
  106.0 17.6 %all_to_all.27.mixed = bf16[32,8,128]{2,1,0:T(8,128)(2,1)S(1)} all-to-all(bf16[32,8,128]{2,1,0:T(8,128)(2,1)S(1)} %get-tuple-element.37), channel_id=1, replica_groups=mesh['tp'=32,'dp'=16] {'tp'}, dimensions={0} | all-to-all | bytes 131072 | tf_op jit(solution)/shard_map/all_to_all | solution.py:54
  123.6 0.9 shard_map.169
  (1 shorter events, 0.0 us)
Async XLA Ops:
  31.7 34.6 %collective-permute-start = (bf16[8,128,384]{2,1,0:T(8,128)(2,1)S(1)}, bf16[8,128,384]{2,1,0:T(8,128)(2,1)S(1)}, u32[]{:S(2)}, u32[]{:S(2)}) collective-permute-start(bf16[8,128,384]{2,1,0:T(8,128)(2,1)S(1)} %all_to_all.25.rest_0_), channel_id=1, source_target_pairs={{0,1},{1,0},{2,3},{3,2},{4,5},{5,4},{6,7},{7,6},{8,9},{9,8},{10,11... | collective-permute-start | bytes 2359304 | tf_op jit(solution)/shard_map/ppermute | solution.py:23
  33.6 3.3 %collective-permute-start.1 = (bf16[128,384]{1,0:T(8,128)(2,1)S(1)}, bf16[128,384]{1,0:T(8,128)(2,1)S(1)}, u32[]{:S(2)}, u32[]{:S(2)}) collective-permute-start(bf16[128,384]{1,0:T(8,128)(2,1)S(1)} %get-tuple-element.30), channel_id=1, source_target_pairs={{0,1},{1,0},{2,3},{3,2},{4,5},{5,4},{6,7},{7,6},{8,9},{9,8},{10,11... | collective-permute-start | bytes 294920 | tf_op jit(solution)/shard_map/ppermute | solution.py:23
  36.9 2.5 %copy-start.3 = (f32[2,4]{1,0:T(2,128)S(1)}, f32[2,4]{1,0:T(2,128)}, u32[]{:S(2)}) copy-start(f32[2,4]{1,0:T(2,128)} %param.21) | copy-start | bytes 100
  37.0 20.4 %collective-permute-start.2 = (bf16[2,128,384]{2,1,0:T(8,128)(2,1)S(1)}, bf16[2,128,384]{2,1,0:T(8,128)(2,1)S(1)}, u32[]{:S(2)}, u32[]{:S(2)}) collective-permute-start(bf16[2,128,384]{2,1,0:T(8,128)(2,1)S(1)} %pad_maximum_fusion.1.rest_0_), channel_id=1, source_target_pairs={{0,2},{2,4},{4,6},{6,8},{8,10},{10,12},{12,14},{14,0},{1,15},{3,1}... | collective-permute-start | bytes 589832 | tf_op jit(solution)/shard_map/ppermute | solution.py:35
  40.1 3.1 %copy-start.2 = (bf16[16,128]{1,0:T(8,128)(2,1)S(1)}, bf16[16,128]{1,0:T(8,128)(2,1)}, u32[]{:S(2)}) copy-start(bf16[16,128]{1,0:T(8,128)(2,1)} %before.1) | copy-start | bytes 12292
  41.6 0.8 copy-start
  42.4 0.8 copy-start.1
  43.9 22.3 %all-to-all-start = ((bf16[32,16,128]{2,1,0:T(8,128)(2,1)}), bf16[32,16,128]{2,1,0:T(8,128)(2,1)S(1)}, u32[]{:S(2)}, u32[]{:S(2)}) async-start(bf16[32,16,128]{2,1,0:T(8,128)(2,1)} %copy_step.1), calls=%async_computation | async-start | bytes 262144 | tf_op jit(solution)/shard_map/all_to_all | solution.py:54
  57.4 10.8 %collective-permute-start.3 = (bf16[2,128,384]{2,1,0:T(8,128)(2,1)S(1)}, bf16[2,128,384]{2,1,0:T(8,128)(2,1)S(1)}, u32[]{:S(2)}, u32[]{:S(2)}) collective-permute-start(bf16[2,128,384]{2,1,0:T(8,128)(2,1)S(1)} %collective-permute-done.2.rest_1_), channel_id=1, source_target_pairs={{0,2},{2,4},{4,6},{6,8},{8,10},{10,12},{12,14},{14,0},{1,15},{3,1}... | collective-permute-start | bytes 589832 | tf_op jit(solution)/shard_map/ppermute | solution.py:35
  68.1 19.2 %collective-permute-start.4 = (bf16[2,128,384]{2,1,0:T(8,128)(2,1)S(1)}, bf16[2,128,384]{2,1,0:T(8,128)(2,1)S(1)}, u32[]{:S(2)}, u32[]{:S(2)}) collective-permute-start(bf16[2,128,384]{2,1,0:T(8,128)(2,1)S(1)} %collective-permute-done.3.rest_2_), channel_id=1, source_target_pairs={{0,2},{2,4},{4,6},{6,8},{8,10},{10,12},{12,14},{14,0},{1,15},{3,1}... | collective-permute-start | bytes 589832 | tf_op jit(solution)/shard_map/ppermute | solution.py:35
  87.4 16.6 %collective-permute-start.6 = (bf16[6,128,384]{2,1,0:T(8,128)(2,1)S(1)}, bf16[6,128,384]{2,1,0:T(8,128)(2,1)S(1)}, u32[]{:S(2)}, u32[]{:S(2)}) collective-permute-start(bf16[6,128,384]{2,1,0:T(8,128)(2,1)S(1)} %pad_maximum_fusion), channel_id=1, source_target_pairs={{0,1},{1,0},{2,3},{3,2},{4,5},{5,4},{6,7},{7,6},{8,9},{9,8},{10,11... | collective-permute-start | bytes 1769480 | tf_op jit(solution)/shard_map/ppermute | solution.py:23
  89.3 14.7 %all-to-all-start.3 = ((bf16[32,16,128]{2,1,0:T(8,128)(2,1)}), bf16[32,16,128]{2,1,0:T(8,128)(2,1)S(1)}, u32[]{:S(2)}, u32[]{:S(2)}) async-start(bf16[32,16,128]{2,1,0:T(8,128)(2,1)} %get-tuple-element.29), calls=%async_computation.3 | async-start | bytes 262144 | tf_op jit(solution)/shard_map/all_to_all | solution.py:54
  94.4 9.6 %collective-permute-start.5 = (bf16[2,128,384]{2,1,0:T(8,128)(2,1)S(1)}, bf16[2,128,384]{2,1,0:T(8,128)(2,1)S(1)}, u32[]{:S(2)}, u32[]{:S(2)}) collective-permute-start(bf16[2,128,384]{2,1,0:T(8,128)(2,1)S(1)} %collective-permute-done.4.rest_3_), channel_id=1, source_target_pairs={{0,2},{2,4},{4,6},{6,8},{8,10},{10,12},{12,14},{14,0},{1,15},{3,1}... | collective-permute-start | bytes 589832 | tf_op jit(solution)/shard_map/ppermute | solution.py:35
where the time goes:
time: 125 us; the launch traced here: 124 us
  blocking collectives  63.3 us (51%)
  starting transfers between devices  33.5 us (27%)
  waiting for transfers between devices  15.6 us (12%)
  Pallas kernels  8.91 us (7%)
  local copies, waits for them, and re-layouts  2.28 us (2%)
    all_to_all x2, blocking collectives, over_tp(): return lax.all_to_all(copies, 'tp', split_axis=0, concat_axis=0, tiled=True)  33.3 us
    all_to_all x1, blocking collectives, along_y(): lax.all_to_all(copies, 'dp', split_axis=0, concat_axis=0, tiled=True, axi...  30 us
    all_to_all x2, starting transfers between devices, over_tp(): return lax.all_to_all(copies, 'tp', split_axis=0, concat_axis=0, tiled=True)  18.5 us
    all_to_all x2, waiting for transfers between devices, over_tp(): return lax.all_to_all(copies, 'tp', split_axis=0, concat_axis=0, tiled=True)  14.6 us
    ppermute x4, starting transfers between devices, round_step(): return lax.ppermute(piece, 'dp', ROUND)  8.74 us
    ppermute x3, starting transfers between devices, to_partner(): return lax.ppermute(array, 'dp', PARTNER)  6.24 us
    pallas_call x2, Pallas kernels, mixer_call(): pl.pallas_call(functools.partial(mixer_kernel, layer), in_specs=specs, ou...  3.88 us
  transfers between devices with their start and end apart: 9, of which 3 were waited for; matrix products, arithmetic and copies ran while one was open for 1% of the time, Pallas kernels for 4%

commit v1 on v0

--- a/solution.py
+++ b/solution.py
@@ -15,39 +15,31 @@
 
 
 PARTNER = [(i, i ^ 1) for i in range(16)]
-SAME_CORE = [[2 * y + c for y in range(8)] for c in range(2)]
-ROUND = [(2 * y, 2 * ((y + 1) % 8)) for y in range(8)] + [(2 * y + 1, 2 * ((y - 1) % 8) + 1) for y in range(8)]
 
 
 def to_partner(array):
     return lax.ppermute(array, "dp", PARTNER)
 
 
-def along_y(copies):
-    return lax.all_to_all(copies, "dp", split_axis=0, concat_axis=0, tiled=True, axis_index_groups=SAME_CORE)
+def from_y(array, k):
+    pairs = [(2 * ((y + k) % 8), 2 * y) for y in range(8)] + [(2 * ((y - k) % 8) + 1, 2 * y + 1) for y in range(8)]
+    return lax.ppermute(array, "dp", pairs)
 
 
 def behind(array, *others):
     return lax.optimization_barrier((array, *others))[0]
 
 
-def round_step(piece):
-    return lax.ppermute(piece, "dp", ROUND)
-
-
-def block_of(here, i):
+def shards_of(here, pieces):
     y, c = here >> 1, here & 1
-    k = i // 2
-    step = k if k < 5 else 4 - k
-    core = c if (i % 2 == 1) == (k >= 5) else 1 - c
-    return 2 * ((y + (2 * c - 1) * step) & 7) + core
-
-
-def shards_of(layer, here, pieces):
-    if layer == 0:
-        return [(2 * (i % 8) + ((here & 1) ^ (i // 8)), pieces[i // 8], i % 8) for i in range(16)]
-    ring = [(block_of(here, i), pieces[i // 2], i % 2) for i in range(10)]
-    return ring + [(block_of(here, i), pieces[5], i - 10) for i in range(10, 16)]
+    way = 1 - 2 * c
+    order = [(0, 0, 0), (0, 2, 1), (1, 0, 2), (1, 2, 3), (2, 0, 4), (3, 0, -1), (3, 2, -2), (3, 4, -3)]
+    found = []
+    for array, at, k in order:
+        first = c if array < 3 else 1 - c
+        base = 2 * ((y + way * k) & 7)
+        found += [(base + first, pieces[array], at), (base + 1 - first, pieces[array], at + 1)]
+    return found
 
 
 def over_tp(copies):
@@ -68,18 +60,26 @@
     return body
 
 
-def send_kernel(w_in, w_gate, w_out, first, second):
-    for y in range(8):
-        first[y, 0:64, 0:256] = w_in[0]
-        first[y, 64:128, 0:256] = w_gate[0]
-        first[y, :, 256:384] = w_out[0]
-    second[0:64, 0:256] = w_in[1]
-    second[64:128, 0:256] = w_gate[1]
-    second[:, 256:384] = w_out[1]
-
-
-def copy_kernel(tokens, *rest):
-    rest[-1][...] = jnp.broadcast_to(tokens[...][None], rest[-1].shape)
+def send_kernel(w_in, w_gate, w_out, shard):
+    for l in range(2):
+        at = 384 * l
+        shard[0, 0:64, at : at + 256] = w_in[l]
+        shard[0, 64:128, at : at + 256] = w_gate[l]
+        shard[0, :, at + 256 : at + 384] = w_out[l]
+
+
+def stack_kernel(pair, near, tokens, both0, both1, copies):
+    for l, both in ((0, both0), (1, both1)):
+        lanes = slice(384 * l, 384 * l + 384)
+        both[0:2] = pair[:, :, lanes]
+        both[2:4] = near[:, :, lanes]
+    copies[...] = jnp.broadcast_to(tokens[...][None], copies.shape)
+
+
+def join_kernel(both, far, joined, last):
+    joined[0:2] = both[2:4]
+    joined[2:6] = far[...]
+    last[...] = far[2:4]
 
 
 def prepare_kernel(gains, decay_rate, frequency, log_step, map_re, map_im, read_re, read_im, skip_weight, state_re, state_im, gain, drive, read, decay, skip, old):
@@ -123,7 +123,7 @@
     square = jnp.sum(jnp.sum(wide * wide, axis=0), axis=1, keepdims=True)
     inv_scale = lax.rsqrt(square * (1.0 / 4096) + EPSILON)
     total = jnp.zeros((16, 128), F32)
-    for block, array, at in shards_of(layer, here[0], pieces):
+    for block, array, at in shards_of(here[0], pieces):
         t = 2 * block
         left = (x[t].astype(F32) * inv_scale * gain[layer, pl.ds(t, 1), :]).astype(BF16)
         right = (x[t + 1].astype(F32) * inv_scale * gain[layer, pl.ds(t + 1, 1), :]).astype(BF16)
@@ -148,11 +148,10 @@
 
 
 def out_kernel(layer, here, mixed, before, *rest):
-    count = 2 if layer == 0 else 6
-    pieces, outs = rest[:count], rest[count:]
+    pieces, outs = rest[:4], rest[4:]
     low = lax.broadcasted_iota(jnp.int32, (8, 128), 1) < 64
     total = jnp.zeros((16, 128), F32)
-    for block, array, at in shards_of(layer, here[0], pieces):
+    for block, array, at in shards_of(here[0], pieces):
         t = 2 * block
         a = mixed[t].astype(F32)
         b = mixed[t + 1].astype(F32)
@@ -221,48 +220,41 @@
     )(*args)
 
 
-def copy_call(tokens, *after):
-    return pl.pallas_call(
-        copy_kernel,
-        in_specs=[VMEM] + [pl.BlockSpec(memory_space=pl.ANY)] * len(after),
-        out_specs=VMEM,
-        out_shape=jax.ShapeDtypeStruct((32, 16, 128), BF16),
-        compiler_params=pltpu.CompilerParams(vmem_limit_bytes=16 << 20),
-        name="copy_step",
-    )(tokens, *after)
-
-
 def local(tokens, norm_gain, w_in, w_gate, decay_rate, frequency, log_step, map_re, map_im, read_re, read_im, skip_weight, w_out, state_re, state_im):
     here = lax.axis_index("dp").astype(jnp.int32).reshape(1)
-    first, second = run_loaded(
-        send_kernel,
-        (w_in.transpose(0, 2, 1), w_gate.transpose(0, 2, 1), w_out),
-        [((8, 128, 384), BF16), ((128, 384), BF16)],
-        (1,),
-    )
+    shard = run_loaded(
+        send_kernel, (w_in.transpose(0, 2, 1), w_gate.transpose(0, 2, 1), w_out), [((1, 128, 768), BF16)], (0,)
+    )[0]
     small = run_loaded(
         prepare_kernel,
         (norm_gain, decay_rate, frequency, log_step[:, :, None], map_re, map_im, read_re, read_im, skip_weight, state_re, state_im),
         [((2, 32, 128), F32), ((2, 128, 512), F32), ((2, 128, 512), F32), ((2, 2, 256), F32), ((2, 1, 128), F32), ((2, 2, 16, 256), F32)],
         (0, 3, 4, 5),
     )
-    w_own = along_y(first)
-    pieces = [jnp.stack([second, to_partner(second)])]
-    pieces.append(round_step(pieces[0]))
-    w_other = to_partner(w_own)
-    copies = copy_call(tokens, small[3])
+    pair = jnp.concatenate([shard, to_partner(shard)])
+    near = from_y(pair, 1)
+    shapes = [((4, 128, 384), BF16)] * 2 + [((32, 16, 128), BF16)]
+    both0, both1, copies = run(stack_kernel, close(pair, near) + [tokens], shapes, range(2))
+
+    def pieces_of(both):
+        far = from_y(both, 2)
+        shapes = [((6, 128, 384), BF16), ((2, 128, 384), BF16)]
+        joined, last = run(join_kernel, close(both, far), shapes, (0, 1))
+        last = from_y(last, 1)
+        across = to_partner(joined)
+        return [both, far, last, across]
+
     gathered = over_tp(copies)
-    pieces.append(round_step(behind(pieces[1], w_own)))
-    mixed, fresh0 = mixer_call(0, here, gathered, small, (w_own, w_other))
-    pieces.append(round_step(behind(pieces[2], fresh0)))
+    first = pieces_of(both0)
+    mixed, fresh0 = mixer_call(0, here, gathered, small, first)
+    second = pieces_of(behind(both1, fresh0))
     mixed = over_tp(mixed)
     shapes = [((16, 128), BF16), ((32, 16, 128), BF16)]
-    hidden, copies = run(functools.partial(out_kernel, 0), (here, *close(mixed), tokens, *close(w_own, w_other)), shapes, (0,), 1)
-    pieces.append(round_step(behind(pieces[3], hidden)))
-    pieces.append(to_partner(behind(jnp.concatenate(pieces[1:4]), hidden)))
-    mixed, fresh1 = mixer_call(1, here, over_tp(copies), small, pieces)
+    hidden, copies = run(functools.partial(out_kernel, 0), (here, *close(mixed), tokens, *close(*first)), shapes, (0,), 1)
+    gathered = over_tp(copies)
+    mixed, fresh1 = mixer_call(1, here, gathered, small, second)
     shapes = [((16, 128), BF16), (state_re.shape, F32), (state_im.shape, F32)]
-    args = (here, *close(over_tp(mixed), hidden, *pieces, fresh0, fresh1))
+    args = (here, *close(over_tp(mixed), hidden, *second, fresh0, fresh1))
     return tuple(run(functools.partial(out_kernel, 1), args, shapes, (), 1))
 
 

time: 125 us -> 133 us (1.064)
  the two profiles are of different devices: /device:TPU:2 before, /device:TPU:24 now
where the time goes in v1:
time: 133 us; the launch traced here: 132 us
  waiting for transfers between devices  46.7 us (35%)
  blocking collectives  36.4 us (27%)
  starting transfers between devices  35.2 us (26%)
  Pallas kernels  9.97 us (7%)
  local copies, waits for them, and re-layouts  2.98 us (2%)
    all_to_all x2, blocking collectives, over_tp(): return lax.all_to_all(copies, 'tp', split_axis=0, concat_axis=0, tiled=True)  36.4 us
    ppermute x5, waiting for transfers between devices, from_y(): return lax.ppermute(array, 'dp', pairs)  31.9 us
    all_to_all x2, starting transfers between devices, over_tp(): return lax.all_to_all(copies, 'tp', split_axis=0, concat_axis=0, tiled=True)  17 us
    all_to_all x2, waiting for transfers between devices, over_tp(): return lax.all_to_all(copies, 'tp', split_axis=0, concat_axis=0, tiled=True)  13.3 us
    ppermute x5, starting transfers between devices, from_y(): return lax.ppermute(array, 'dp', pairs)  12.5 us
    ppermute x3, starting transfers between devices, to_partner(): return lax.ppermute(array, 'dp', PARTNER)  5.75 us
    pallas_call x2, Pallas kernels, mixer_call(): pl.pallas_call(functools.partial(mixer_kernel, layer), in_specs=specs, ou...  4 us
    pallas_call x5, Pallas kernels, run(): pl.pallas_call(kernel, in_specs=[SMEM] * smem + [VMEM] * (len(args) - sme...  3.57 us
  transfers between devices with their start and end apart: 10, of which 6 were waited for; matrix products, arithmetic and copies ran while one was open for 1% of the time, Pallas kernels for 2%

profile of v1, /device:TPU:24, one launch (start us, length us, event | category | flops | bytes accessed | tf_op | source)
XLA Modules:
  0.0 132.1 jit_solution(87950629574362573)
XLA Ops:
  0.6 0.9 shard_map.166
  1.6 0.0 copy-start.2
  1.6 1.9 %collective-permute-start = (bf16[1,128,768]{2,1,0:T(8,128)(2,1)S(1)}, bf16[1,128,768]{2,1,0:T(8,128)(2,1)S(1)}, u32[]{:S(2)}, u32[]{:S(2)}) collective-permute-start(bf16[1,128,768]{2,1,0:T(8,128)(2,1)S(1)} %shard_map.166), channel_id=1, source_target_pairs={{0,1},{1,0},{2,3},{3,2},{4,5},{5,4},{6,7},{7,6},{8,9},{9,8},{10,11... | collective-permute-start | bytes 589832 | tf_op jit(solution)/shard_map/ppermute | solution.py:21
  3.5 1.4 %collective-permute-done = bf16[1,128,768]{2,1,0:T(8,128)(2,1)S(1)} collective-permute-done((bf16[1,128,768]{2,1,0:T(8,128)(2,1)S(1)}, bf16[1,128,768]{2,1,0:T(8,128)(2,1)S(1)}, u32[]{:S(2)}, u32[]{:S(2)}) %collective-permute-start) | collective-permute-done | bytes 196640 | tf_op jit(solution)/shard_map/ppermute | solution.py:21
  5.0 2.4 %collective-permute-start.1 = (bf16[2,128,768]{2,1,0:T(8,128)(2,1)S(1)}, bf16[2,128,768]{2,1,0:T(8,128)(2,1)S(1)}, u32[]{:S(2)}, u32[]{:S(2)}) collective-permute-start(bf16[2,128,768]{2,1,0:T(8,128)(2,1)S(1)} %pad_maximum_fusion.pair), channel_id=1, source_target_pairs={{2,0},{4,2},{6,4},{8,6},{10,8},{12,10},{14,12},{0,14},{15,1},{1,3}... | collective-permute-start | bytes 1179656 | tf_op jit(solution)/shard_map/ppermute | solution.py:26
  7.3 8.5 %collective-permute-done.1.near = bf16[2,128,768]{2,1,0:T(8,128)(2,1)S(1)} collective-permute-done((bf16[2,128,768]{2,1,0:T(8,128)(2,1)S(1)}, bf16[2,128,768]{2,1,0:T(8,128)(2,1)S(1)}, u32[]{:S(2)}, u32[]{:S(2)}) %collective-permute-start.1) | collective-permute-done | bytes 393248 | tf_op jit(solution)/shard_map/ppermute | solution.py:26
  15.9 0.0 copy-done.2
  15.9 0.7 shard_map.167
  16.6 4.3 %collective-permute-start.2 = (bf16[4,128,384]{2,1,0:T(8,128)(2,1)S(1)}, bf16[4,128,384]{2,1,0:T(8,128)(2,1)S(1)}, u32[]{:S(2)}, u32[]{:S(2)}) collective-permute-start(bf16[4,128,384]{2,1,0:T(8,128)(2,1)S(1)} %get-tuple-element.30.both.rest_0_), channel_id=1, source_target_pairs={{4,0},{6,2},{8,4},{10,6},{12,8},{14,10},{0,12},{2,14},{13,1},{15,3... | collective-permute-start | bytes 1179656 | tf_op jit(solution)/shard_map/ppermute | solution.py:26
  20.9 11.5 %collective-permute-done.2.far.rest_1_ = bf16[4,128,384]{2,1,0:T(8,128)(2,1)S(1)} collective-permute-done((bf16[4,128,384]{2,1,0:T(8,128)(2,1)S(1)}, bf16[4,128,384]{2,1,0:T(8,128)(2,1)S(1)}, u32[]{:S(2)}, u32[]{:S(2)}) %collective-permute-start.2) | collective-permute-done | bytes 393248 | tf_op jit(solution)/shard_map/ppermute | solution.py:26
  32.4 0.1 shard_map.169
  32.5 1.9 %collective-permute-start.4 = (bf16[6,128,384]{2,1,0:T(8,128)(2,1)S(1)}, bf16[6,128,384]{2,1,0:T(8,128)(2,1)S(1)}, u32[]{:S(2)}, u32[]{:S(2)}) collective-permute-start(bf16[6,128,384]{2,1,0:T(8,128)(2,1)S(1)} %get-tuple-element.32), channel_id=1, source_target_pairs={{0,1},{1,0},{2,3},{3,2},{4,5},{5,4},{6,7},{7,6},{8,9},{9,8},{10,11... | collective-permute-start | bytes 1769480 | tf_op jit(solution)/shard_map/ppermute | solution.py:21
  34.4 13.2 %all-to-all-start = ((bf16[32,16,128]{2,1,0:T(8,128)(2,1)}), bf16[32,16,128]{2,1,0:T(8,128)(2,1)S(1)}, u32[]{:S(2)}, u32[]{:S(2)}) async-start(bf16[32,16,128]{2,1,0:T(8,128)(2,1)} %get-tuple-element.23), calls=%async_computation | async-start | bytes 262144 | tf_op jit(solution)/shard_map/all_to_all | solution.py:46
  47.6 1.9 %collective-permute-start.3 = (bf16[2,128,384]{2,1,0:T(8,128)(2,1)S(1)}, bf16[2,128,384]{2,1,0:T(8,128)(2,1)S(1)}, u32[]{:S(2)}, u32[]{:S(2)}) collective-permute-start(bf16[2,128,384]{2,1,0:T(8,128)(2,1)S(1)} %get-tuple-element.31), channel_id=1, source_target_pairs={{2,0},{4,2},{6,4},{8,6},{10,8},{12,10},{14,12},{0,14},{15,1},{1,3}... | collective-permute-start | bytes 589832 | tf_op jit(solution)/shard_map/ppermute | solution.py:26
  49.6 0.0 copy-start.3
  49.6 0.7 copy-done.3
  50.2 0.7 copy.18.refs_3_
  50.9 1.5 %shard_map.168 = (f32[2,32,128]{2,1,0:T(8,128)S(1)}, f32[2,128,512]{2,1,0:T(8,128)S(1)}, f32[2,128,512]{2,1,0:T(8,128)S(1)}, f32[2,2,256]{2,1,0:T(2,128)S(1)}, f...) custom-call(f32[2,4096]{1,0:T(2,128)} %refs_0_.1, f32[2,4,64]{2,1,0:T(4,128)} %refs_1_.1, f32[2,4,64]{2,1,0:T(4,128)} %refs_2_.3, ...), custom_call_target="tpu_custom_call" | custom-call | tf_op jit(solution)/shard_map/pallas_call | solution.py:195
  52.4 0.0 copy-start
  52.4 0.8 copy-done
  53.2 0.0 copy-start.1
  53.2 0.8 copy-done.1
  54.0 4.7 %all-to-all-done.x = bf16[32,16,128]{2,1,0:T(8,128)(2,1)S(1)} async-done(((bf16[32,16,128]{2,1,0:T(8,128)(2,1)}), bf16[32,16,128]{2,1,0:T(8,128)(2,1)S(1)}, u32[]{:S(2)}, u32[]{:S(2)}) %all-to-all-start) | async-done | bytes 131104 | tf_op jit(solution)/shard_map/all_to_all | solution.py:46
  58.7 0.0 collective-permute-done.3.rest_2_
  58.7 0.0 collective-permute-done.4.rest_3_
  58.7 2.0 %mixer_step.2 = (bf16[32,8,128]{2,1,0:T(8,128)(2,1)S(1)}, f32[16,512]{1,0:T(8,128)S(1)}) custom-call(s32[1]{0:T(128)} %bitcast.here, bf16[32,16,128]{2,1,0:T(8,128)(2,1)S(1)} %all-to-all-done.x, f32[2,32,128]{2,1,0:T(8,128)S(1)} %get-tuple-element.24.gain, f32[2,128,512]{2,1,0:T(8,128)} %copy-done, f32[2,128,512]{2,1,0:T(8,128)} %copy-done.1, ...), custom_call_target="tpu_custom_call" | custom-call | tf_op jit(solution)/shard_map/mixer_step/pallas_call | solution.py:212
  60.7 1.9 %collective-permute-start.5 = (bf16[4,128,384]{2,1,0:T(8,128)(2,1)S(1)}, bf16[4,128,384]{2,1,0:T(8,128)(2,1)S(1)}, u32[]{:S(2)}, u32[]{:S(2)}) collective-permute-start(bf16[4,128,384]{2,1,0:T(8,128)(2,1)S(1)} %get-tuple-element.37.both.rest_0_), channel_id=1, source_target_pairs={{4,0},{6,2},{8,4},{10,6},{12,8},{14,10},{0,12},{2,14},{13,1},{15,3... | collective-permute-start | bytes 1179656 | tf_op jit(solution)/shard_map/ppermute | solution.py:26
  62.6 11.9 %collective-permute-done.5.far.rest_1_ = bf16[4,128,384]{2,1,0:T(8,128)(2,1)S(1)} collective-permute-done((bf16[4,128,384]{2,1,0:T(8,128)(2,1)S(1)}, bf16[4,128,384]{2,1,0:T(8,128)(2,1)S(1)}, u32[]{:S(2)}, u32[]{:S(2)}) %collective-permute-start.5) | collective-permute-done | bytes 393248 | tf_op jit(solution)/shard_map/ppermute | solution.py:26
  74.6 0.9 shard_map.171
  75.4 1.9 %collective-permute-start.7 = (bf16[6,128,384]{2,1,0:T(8,128)(2,1)}, bf16[6,128,384]{2,1,0:T(8,128)(2,1)S(1)}, u32[]{:S(2)}, u32[]{:S(2)}) collective-permute-start(bf16[6,128,384]{2,1,0:T(8,128)(2,1)} %get-tuple-element.39), channel_id=1, source_target_pairs={{0,1},{1,0},{2,3},{3,2},{4,5},{5,4},{6,7},{7,6},{8,9},{9,8},{10,11... | collective-permute-start | bytes 1769480 | tf_op jit(solution)/shard_map/ppermute | solution.py:21
  77.4 18.7 %all_to_all.20.mixed = bf16[32,8,128]{2,1,0:T(8,128)(2,1)S(1)} all-to-all(bf16[32,8,128]{2,1,0:T(8,128)(2,1)S(1)} %get-tuple-element.33), channel_id=1, replica_groups=mesh['tp'=32,'dp'=16] {'tp'}, dimensions={0} | all-to-all | bytes 131072 | tf_op jit(solution)/shard_map/all_to_all | solution.py:46
  96.0 1.0 shard_map.170
  97.0 3.8 %all-to-all-start.2 = ((bf16[32,16,128]{2,1,0:T(8,128)(2,1)}), bf16[32,16,128]{2,1,0:T(8,128)(2,1)S(1)}, u32[]{:S(2)}, u32[]{:S(2)}) async-start(bf16[32,16,128]{2,1,0:T(8,128)(2,1)} %get-tuple-element.34), calls=%async_computation.2 | async-start | bytes 262144 | tf_op jit(solution)/shard_map/all_to_all | solution.py:46
  100.8 1.9 %collective-permute-start.6 = (bf16[2,128,384]{2,1,0:T(8,128)(2,1)S(1)}, bf16[2,128,384]{2,1,0:T(8,128)(2,1)S(1)}, u32[]{:S(2)}, u32[]{:S(2)}) collective-permute-start(bf16[2,128,384]{2,1,0:T(8,128)(2,1)S(1)} %get-tuple-element.38), channel_id=1, source_target_pairs={{2,0},{4,2},{6,4},{8,6},{10,8},{12,10},{14,12},{0,14},{15,1},{1,3}... | collective-permute-start | bytes 589832 | tf_op jit(solution)/shard_map/ppermute | solution.py:26
  102.8 8.6 %all-to-all-done.2.x = bf16[32,16,128]{2,1,0:T(8,128)(2,1)S(1)} async-done(((bf16[32,16,128]{2,1,0:T(8,128)(2,1)}), bf16[32,16,128]{2,1,0:T(8,128)(2,1)S(1)}, u32[]{:S(2)}, u32[]{:S(2)}) %all-to-all-start.2) | async-done | bytes 131104 | tf_op jit(solution)/shard_map/all_to_all | solution.py:46
  111.4 0.0 collective-permute-done.6.rest_2_
  111.4 0.0 collective-permute-done.7.rest_3_
  111.4 2.0 %mixer_step.3 = (bf16[32,8,128]{2,1,0:T(8,128)(2,1)S(1)}, f32[16,512]{1,0:T(8,128)S(1)}) custom-call(s32[1]{0:T(128)} %bitcast.here, bf16[32,16,128]{2,1,0:T(8,128)(2,1)S(1)} %all-to-all-done.2.x, f32[2,32,128]{2,1,0:T(8,128)S(1)} %get-tuple-element.24.gain, f32[2,128,512]{2,1,0:T(8,128)} %copy-done, f32[2,128,512]{2,1,0:T(8,128)} %copy-done.1, ...), custom_call_target="tpu_custom_call" | custom-call | tf_op jit(solution)/shard_map/mixer_step/pallas_call | solution.py:212
  113.4 17.8 %all_to_all.21.mixed = bf16[32,8,128]{2,1,0:T(8,128)(2,1)S(1)} all-to-all(bf16[32,8,128]{2,1,0:T(8,128)(2,1)S(1)} %get-tuple-element.40), channel_id=1, replica_groups=mesh['tp'=32,'dp'=16] {'tp'}, dimensions={0} | all-to-all | bytes 131072 | tf_op jit(solution)/shard_map/all_to_all | solution.py:46
  131.2 0.9 shard_map.172
  (1 shorter events, 0.0 us)
Async XLA Ops:
  1.6 14.3 %copy-start.2 = (bf16[16,128]{1,0:T(8,128)(2,1)S(1)}, bf16[16,128]{1,0:T(8,128)(2,1)}, u32[]{:S(2)}) copy-start(bf16[16,128]{1,0:T(8,128)(2,1)} %before.1) | copy-start | bytes 12292
  1.6 3.3 %collective-permute-start = (bf16[1,128,768]{2,1,0:T(8,128)(2,1)S(1)}, bf16[1,128,768]{2,1,0:T(8,128)(2,1)S(1)}, u32[]{:S(2)}, u32[]{:S(2)}) collective-permute-start(bf16[1,128,768]{2,1,0:T(8,128)(2,1)S(1)} %shard_map.166), channel_id=1, source_target_pairs={{0,1},{1,0},{2,3},{3,2},{4,5},{5,4},{6,7},{7,6},{8,9},{9,8},{10,11... | collective-permute-start | bytes 589832 | tf_op jit(solution)/shard_map/ppermute | solution.py:21
  5.0 10.9 %collective-permute-start.1 = (bf16[2,128,768]{2,1,0:T(8,128)(2,1)S(1)}, bf16[2,128,768]{2,1,0:T(8,128)(2,1)S(1)}, u32[]{:S(2)}, u32[]{:S(2)}) collective-permute-start(bf16[2,128,768]{2,1,0:T(8,128)(2,1)S(1)} %pad_maximum_fusion.pair), channel_id=1, source_target_pairs={{2,0},{4,2},{6,4},{8,6},{10,8},{12,10},{14,12},{0,14},{15,1},{1,3}... | collective-permute-start | bytes 1179656 | tf_op jit(solution)/shard_map/ppermute | solution.py:26
  16.6 15.8 %collective-permute-start.2 = (bf16[4,128,384]{2,1,0:T(8,128)(2,1)S(1)}, bf16[4,128,384]{2,1,0:T(8,128)(2,1)S(1)}, u32[]{:S(2)}, u32[]{:S(2)}) collective-permute-start(bf16[4,128,384]{2,1,0:T(8,128)(2,1)S(1)} %get-tuple-element.30.both.rest_0_), channel_id=1, source_target_pairs={{4,0},{6,2},{8,4},{10,6},{12,8},{14,10},{0,12},{2,14},{13,1},{15,3... | collective-permute-start | bytes 1179656 | tf_op jit(solution)/shard_map/ppermute | solution.py:26
  32.5 26.2 %collective-permute-start.4 = (bf16[6,128,384]{2,1,0:T(8,128)(2,1)S(1)}, bf16[6,128,384]{2,1,0:T(8,128)(2,1)S(1)}, u32[]{:S(2)}, u32[]{:S(2)}) collective-permute-start(bf16[6,128,384]{2,1,0:T(8,128)(2,1)S(1)} %get-tuple-element.32), channel_id=1, source_target_pairs={{0,1},{1,0},{2,3},{3,2},{4,5},{5,4},{6,7},{7,6},{8,9},{9,8},{10,11... | collective-permute-start | bytes 1769480 | tf_op jit(solution)/shard_map/ppermute | solution.py:21
  34.4 24.3 %all-to-all-start = ((bf16[32,16,128]{2,1,0:T(8,128)(2,1)}), bf16[32,16,128]{2,1,0:T(8,128)(2,1)S(1)}, u32[]{:S(2)}, u32[]{:S(2)}) async-start(bf16[32,16,128]{2,1,0:T(8,128)(2,1)} %get-tuple-element.23), calls=%async_computation | async-start | bytes 262144 | tf_op jit(solution)/shard_map/all_to_all | solution.py:46
  47.6 11.1 %collective-permute-start.3 = (bf16[2,128,384]{2,1,0:T(8,128)(2,1)S(1)}, bf16[2,128,384]{2,1,0:T(8,128)(2,1)S(1)}, u32[]{:S(2)}, u32[]{:S(2)}) collective-permute-start(bf16[2,128,384]{2,1,0:T(8,128)(2,1)S(1)} %get-tuple-element.31), channel_id=1, source_target_pairs={{2,0},{4,2},{6,4},{8,6},{10,8},{12,10},{14,12},{0,14},{15,1},{1,3}... | collective-permute-start | bytes 589832 | tf_op jit(solution)/shard_map/ppermute | solution.py:26
  49.6 0.7 copy-start.3
  52.4 0.8 copy-start
  53.2 0.8 copy-start.1
  60.7 13.9 %collective-permute-start.5 = (bf16[4,128,384]{2,1,0:T(8,128)(2,1)S(1)}, bf16[4,128,384]{2,1,0:T(8,128)(2,1)S(1)}, u32[]{:S(2)}, u32[]{:S(2)}) collective-permute-start(bf16[4,128,384]{2,1,0:T(8,128)(2,1)S(1)} %get-tuple-element.37.both.rest_0_), channel_id=1, source_target_pairs={{4,0},{6,2},{8,4},{10,6},{12,8},{14,10},{0,12},{2,14},{13,1},{15,3... | collective-permute-start | bytes 1179656 | tf_op jit(solution)/shard_map/ppermute | solution.py:26
  75.4 36.0 %collective-permute-start.7 = (bf16[6,128,384]{2,1,0:T(8,128)(2,1)}, bf16[6,128,384]{2,1,0:T(8,128)(2,1)S(1)}, u32[]{:S(2)}, u32[]{:S(2)}) collective-permute-start(bf16[6,128,384]{2,1,0:T(8,128)(2,1)} %get-tuple-element.39), channel_id=1, source_target_pairs={{0,1},{1,0},{2,3},{3,2},{4,5},{5,4},{6,7},{7,6},{8,9},{9,8},{10,11... | collective-permute-start | bytes 1769480 | tf_op jit(solution)/shard_map/ppermute | solution.py:21
  97.0 14.4 %all-to-all-start.2 = ((bf16[32,16,128]{2,1,0:T(8,128)(2,1)}), bf16[32,16,128]{2,1,0:T(8,128)(2,1)S(1)}, u32[]{:S(2)}, u32[]{:S(2)}) async-start(bf16[32,16,128]{2,1,0:T(8,128)(2,1)} %get-tuple-element.34), calls=%async_computation.2 | async-start | bytes 262144 | tf_op jit(solution)/shard_map/all_to_all | solution.py:46
  100.8 10.6 %collective-permute-start.6 = (bf16[2,128,384]{2,1,0:T(8,128)(2,1)S(1)}, bf16[2,128,384]{2,1,0:T(8,128)(2,1)S(1)}, u32[]{:S(2)}, u32[]{:S(2)}) collective-permute-start(bf16[2,128,384]{2,1,0:T(8,128)(2,1)S(1)} %get-tuple-element.38), channel_id=1, source_target_pairs={{2,0},{4,2},{6,4},{8,6},{10,8},{12,10},{14,12},{0,14},{15,1},{1,3}... | collective-permute-start | bytes 589832 | tf_op jit(solution)/shard_map/ppermute | solution.py:26

commit v2 on v1

--- a/solution.py
+++ b/solution.py
@@ -9,7 +9,6 @@
 
 
 EPSILON = 1e-06
-HIGH = lax.Precision.HIGHEST
 F32 = jnp.float32
 BF16 = jnp.bfloat16
 
@@ -24,10 +23,6 @@
 def from_y(array, k):
     pairs = [(2 * ((y + k) % 8), 2 * y) for y in range(8)] + [(2 * ((y - k) % 8) + 1, 2 * y + 1) for y in range(8)]
     return lax.ppermute(array, "dp", pairs)
-
-
-def behind(array, *others):
-    return lax.optimization_barrier((array, *others))[0]
 
 
 def shards_of(here, pieces):
@@ -46,16 +41,16 @@
     return lax.all_to_all(copies, "tp", split_axis=0, concat_axis=0, tiled=True)
 
 
-def loaded(kernel, count):
+def loaded(kernel, count, outs_count):
     def body(*refs):
-        sources, sems = refs[:count], refs[-1]
-        outs, local = refs[count : -count - 1], refs[-count - 1 : -1]
+        sources, outs = refs[:count], refs[count : count + outs_count]
+        local, sems, own = refs[count + outs_count : 2 * count + outs_count], refs[2 * count + outs_count], refs[2 * count + outs_count + 1 :]
         copies = [pltpu.make_async_copy(a, b, sems.at[i]) for i, (a, b) in enumerate(zip(sources, local))]
         for copy in copies:
             copy.start()
         for copy in copies:
             copy.wait()
-        kernel(*local, *outs)
+        kernel(*local, *outs, *own)
 
     return body
 
@@ -68,12 +63,16 @@
         shard[0, :, at + 256 : at + 384] = w_out[l]
 
 
-def stack_kernel(pair, near, tokens, both0, both1, copies):
+def stack_kernel(pair, near, both0, both1):
     for l, both in ((0, both0), (1, both1)):
         lanes = slice(384 * l, 384 * l + 384)
         both[0:2] = pair[:, :, lanes]
         both[2:4] = near[:, :, lanes]
-    copies[...] = jnp.broadcast_to(tokens[...][None], copies.shape)
+
+
+def halves(array):
+    upper = array.astype(BF16)
+    return upper, (array - upper.astype(F32)).astype(BF16)
 
 
 def join_kernel(both, far, joined, last):
@@ -82,7 +81,8 @@
     last[...] = far[2:4]
 
 
-def prepare_kernel(gains, decay_rate, frequency, log_step, map_re, map_im, read_re, read_im, skip_weight, state_re, state_im, gain, drive, read, decay, skip, old):
+def prepare_kernel(gains, decay_rate, frequency, log_step, map_re, map_im, read_re, read_im, skip_weight, state_re, state_im, tokens, gain, drive_far, read_far, decay, skip, old, copies, drive, read, drive_parts, read_parts, sems):
+    copies[...] = jnp.broadcast_to(tokens[...][None], copies.shape)
     drive[...] = jnp.zeros(drive.shape, F32)
     read[...] = jnp.zeros(read.shape, F32)
     skip[...] = jnp.zeros(skip.shape, F32)
@@ -91,7 +91,11 @@
     for l in range(2):
         lam_re = -decay_rate[l]
         lam_im = frequency[l]
-        step_size = jnp.exp(log_step[l])
+        group = lax.broadcasted_iota(jnp.int32, (4, 64), 0)
+        step_size = jnp.zeros((4, 64), F32)
+        for g in range(4):
+            step_size = jnp.where(group == g, log_step[l : l + 1, g : g + 1], step_size)
+        step_size = jnp.exp(step_size)
         magnitude = jnp.exp(lam_re * step_size)
         decay_re = magnitude * jnp.cos(lam_im * step_size)
         decay_im = magnitude * jnp.sin(lam_im * step_size)
@@ -111,6 +115,13 @@
             skip[l, 0:1, 16 * g : 16 * g + 16] = skip_weight[l, g : g + 1]
             old[l, 0, :, at : at + 64] = state_re[l, :, g, :]
             old[l, 1, :, at : at + 64] = state_im[l, :, g, :]
+    moves = []
+    for i, (full, parts, far) in enumerate(((drive, drive_parts, drive_far), (read, read_parts, read_far))):
+        parts[:, :, 0:512], parts[:, :, 512:1024] = halves(full[...])
+        moves.append(pltpu.make_async_copy(parts, far, sems.at[i]))
+        moves[i].start()
+    for move in moves:
+        move.wait()
 
 
 def mixer_kernel(layer, here, x, gain, drive_far, read_far, decay, skip, old, *rest):
@@ -122,16 +133,17 @@
     wide = x[...].astype(F32)
     square = jnp.sum(jnp.sum(wide * wide, axis=0), axis=1, keepdims=True)
     inv_scale = lax.rsqrt(square * (1.0 / 4096) + EPSILON)
-    total = jnp.zeros((16, 128), F32)
+    turned = jnp.zeros((128, 16), F32)
     for block, array, at in shards_of(here[0], pieces):
         t = 2 * block
         left = (x[t].astype(F32) * inv_scale * gain[layer, pl.ds(t, 1), :]).astype(BF16)
         right = (x[t + 1].astype(F32) * inv_scale * gain[layer, pl.ds(t + 1, 1), :]).astype(BF16)
         rows = jnp.concatenate([left, right], axis=1)
-        total += lax.dot_general(rows, array[at, :, 0:256], (((1,), (1,)), ((), ())), preferred_element_type=F32)
-    both = total.astype(BF16).astype(F32)
+        turned += lax.dot_general(array[at, :, 0:256], rows, (((1,), (1,)), ((), ())), preferred_element_type=F32)
+    both = turned.T.astype(BF16).astype(F32)
     get_drive.wait()
-    push = jnp.dot(both, drive[...], precision=HIGH, preferred_element_type=F32)
+    parts = jnp.dot(both.astype(BF16), drive[...], preferred_element_type=F32)
+    push = parts[:, :512] + parts[:, 512:]
     d_re, d_im = decay[layer, 0:1], decay[layer, 1:2]
     o_re, o_im = old[layer, 0], old[layer, 1]
     f_re = d_re * o_re - d_im * o_im + push[:, :256]
@@ -139,7 +151,10 @@
     fresh = jnp.concatenate([f_re, f_im], axis=1)
     fresh_out[...] = fresh
     get_read.wait()
-    readout = lax.dot_general(fresh, read[...], (((1,), (1,)), ((), ())), precision=HIGH, preferred_element_type=F32)
+    upper, lower = halves(fresh)
+    contract = (((1,), (1,)), ((), ()))
+    parts = lax.dot_general(jnp.concatenate([upper, lower]), read[:, :512], contract, preferred_element_type=F32)
+    readout = parts[:16] + parts[16:] + lax.dot_general(upper, read[:, 512:], contract, preferred_element_type=F32)
     readout = readout + skip[layer] * both
     gate = pltpu.roll(both, 64, axis=1)
     mixer = (jax.nn.gelu(readout) * jax.nn.sigmoid(gate)).astype(BF16).astype(F32)
@@ -190,14 +205,14 @@
     )(*args)
 
 
-def run_loaded(kernel, args, shapes, near=()):
+def run_loaded(kernel, args, shapes, near=(), far=(), scratch=()):
     args = [pltpu.with_memory_space_constraint(a, pltpu.HBM) for a in args]
     return pl.pallas_call(
-        loaded(kernel, len(args)),
+        loaded(kernel, len(args), len(shapes)),
         in_specs=[pl.BlockSpec(memory_space=pltpu.HBM)] * len(args),
-        out_specs=[VMEM] * len(shapes),
-        out_shape=[pltpu.VMEM(*s) if i in near else jax.ShapeDtypeStruct(*s) for i, s in enumerate(shapes)],
-        scratch_shapes=[pltpu.VMEM(a.shape, a.dtype) for a in args] + [pltpu.SemaphoreType.DMA((len(args),))],
+        out_specs=[pl.BlockSpec(memory_space=pltpu.HBM) if i in far else VMEM for i in range(len(shapes))],
+        out_shape=[pltpu.VMEM(*s) if i in near else pltpu.HBM(*s) if i in far else jax.ShapeDtypeStruct(*s) for i, s in enumerate(shapes)],
+        scratch_shapes=[pltpu.VMEM(a.shape, a.dtype) for a in args] + [pltpu.SemaphoreType.DMA((len(args),)), *scratch],
         compiler_params=pltpu.CompilerParams(vmem_limit_bytes=16 << 20),
     )(*args)
 
@@ -214,7 +229,7 @@
         in_specs=specs,
         out_specs=[VMEM] * 2,
         out_shape=[jax.ShapeDtypeStruct((32, 8, 128), BF16), pltpu.VMEM((16, 512), F32)],
-        scratch_shapes=[pltpu.VMEM((128, 512), F32)] * 2 + [pltpu.SemaphoreType.DMA((2,))],
+        scratch_shapes=[pltpu.VMEM((128, 1024), BF16)] * 2 + [pltpu.SemaphoreType.DMA((2,))],
         compiler_params=pltpu.CompilerParams(vmem_limit_bytes=16 << 20),
         name="mixer_step",
     )(*args)
@@ -225,16 +240,17 @@
     shard = run_loaded(
         send_kernel, (w_in.transpose(0, 2, 1), w_gate.transpose(0, 2, 1), w_out), [((1, 128, 768), BF16)], (0,)
     )[0]
-    small = run_loaded(
+    *small, copies = run_loaded(
         prepare_kernel,
-        (norm_gain, decay_rate, frequency, log_step[:, :, None], map_re, map_im, read_re, read_im, skip_weight, state_re, state_im),
-        [((2, 32, 128), F32), ((2, 128, 512), F32), ((2, 128, 512), F32), ((2, 2, 256), F32), ((2, 1, 128), F32), ((2, 2, 16, 256), F32)],
+        (norm_gain, decay_rate, frequency, log_step, map_re, map_im, read_re, read_im, skip_weight, state_re, state_im, tokens),
+        [((2, 32, 128), F32), ((2, 128, 1024), BF16), ((2, 128, 1024), BF16), ((2, 2, 256), F32), ((2, 1, 128), F32), ((2, 2, 16, 256), F32), ((32, 16, 128), BF16)],
         (0, 3, 4, 5),
+        (1, 2),
+        [pltpu.VMEM((2, 128, 512), F32)] * 2 + [pltpu.VMEM((2, 128, 1024), BF16)] * 2 + [pltpu.SemaphoreType.DMA((2,))],
     )
     pair = jnp.concatenate([shard, to_partner(shard)])
     near = from_y(pair, 1)
-    shapes = [((4, 128, 384), BF16)] * 2 + [((32, 16, 128), BF16)]
-    both0, both1, copies = run(stack_kernel, close(pair, near) + [tokens], shapes, range(2))
+    both0, both1 = run(stack_kernel, close(pair, near), [((4, 128, 384), BF16)] * 2, range(2))
 
     def pieces_of(both):
         far = from_y(both, 2)
@@ -247,7 +263,7 @@
     gathered = over_tp(copies)
     first = pieces_of(both0)
     mixed, fresh0 = mixer_call(0, here, gathered, small, first)
-    second = pieces_of(behind(both1, fresh0))
+    second = pieces_of(both1)
     mixed = over_tp(mixed)
     shapes = [((16, 128), BF16), ((32, 16, 128), BF16)]
     hidden, copies = run(functools.partial(out_kernel, 0), (here, *close(mixed), tokens, *close(*first)), shapes, (0,), 1)

time: 133 us -> 124 us (0.932)
  the two profiles are of different devices: /device:TPU:24 before, /device:TPU:56 now
where the time goes in v2:
time: 124 us; the launch traced here: 123 us
  starting transfers between devices  37.8 us (30%)
  blocking collectives  37.1 us (30%)
  waiting for transfers between devices  36.2 us (29%)
  Pallas kernels  11.4 us (9%)
    all_to_all x2, blocking collectives, over_tp(): return lax.all_to_all(copies, 'tp', split_axis=0, concat_axis=0, tiled=True)  37.1 us
    ppermute x5, waiting for transfers between devices, from_y(): return lax.ppermute(array, 'dp', pairs)  26.9 us
    all_to_all x2, starting transfers between devices, over_tp(): return lax.all_to_all(copies, 'tp', split_axis=0, concat_axis=0, tiled=True)  19.5 us
    ppermute x5, starting transfers between devices, from_y(): return lax.ppermute(array, 'dp', pairs)  12.4 us
    all_to_all x2, waiting for transfers between devices, over_tp(): return lax.all_to_all(copies, 'tp', split_axis=0, concat_axis=0, tiled=True)  7.87 us
    ppermute x3, starting transfers between devices, to_partner(): return lax.ppermute(array, 'dp', PARTNER)  5.94 us
    pallas_call x2, Pallas kernels, run_loaded(): pl.pallas_call(loaded(kernel, len(args), len(shapes)), in_specs=[pl.Block...  4.08 us
    pallas_call x5, Pallas kernels, run(): pl.pallas_call(kernel, in_specs=[SMEM] * smem + [VMEM] * (len(args) - sme...  3.8 us
  transfers between devices with their start and end apart: 10, of which 7 were waited for; matrix products, arithmetic and copies ran while one was open for 0% of the time, Pallas kernels for 6%

profile of v2, /device:TPU:56, one launch (start us, length us, event | category | flops | bytes accessed | tf_op | source)
XLA Modules:
  0.0 123.4 jit_solution(233196702122059531)
XLA Ops:
  0.6 0.9 shard_map.167
  1.6 1.9 %collective-permute-start = (bf16[1,128,768]{2,1,0:T(8,128)(2,1)S(1)}, bf16[1,128,768]{2,1,0:T(8,128)(2,1)S(1)}, u32[]{:S(2)}, u32[]{:S(2)}) collective-permute-start(bf16[1,128,768]{2,1,0:T(8,128)(2,1)S(1)} %shard_map.167), channel_id=1, source_target_pairs={{0,1},{1,0},{2,3},{3,2},{4,5},{5,4},{6,7},{7,6},{8,9},{9,8},{10,11... | collective-permute-start | bytes 589832 | tf_op jit(solution)/shard_map/ppermute | solution.py:20
  3.5 1.4 %collective-permute-done = bf16[1,128,768]{2,1,0:T(8,128)(2,1)S(1)} collective-permute-done((bf16[1,128,768]{2,1,0:T(8,128)(2,1)S(1)}, bf16[1,128,768]{2,1,0:T(8,128)(2,1)S(1)}, u32[]{:S(2)}, u32[]{:S(2)}) %collective-permute-start) | collective-permute-done | bytes 196640 | tf_op jit(solution)/shard_map/ppermute | solution.py:20
  5.0 3.3 %collective-permute-start.1 = (bf16[2,128,768]{2,1,0:T(8,128)(2,1)S(1)}, bf16[2,128,768]{2,1,0:T(8,128)(2,1)S(1)}, u32[]{:S(2)}, u32[]{:S(2)}) collective-permute-start(bf16[2,128,768]{2,1,0:T(8,128)(2,1)S(1)} %pad_maximum_fusion.pair), channel_id=1, source_target_pairs={{2,0},{4,2},{6,4},{8,6},{10,8},{12,10},{14,12},{0,14},{15,1},{1,3}... | collective-permute-start | bytes 1179656 | tf_op jit(solution)/shard_map/ppermute | solution.py:25
  8.2 9.5 %collective-permute-done.1.near = bf16[2,128,768]{2,1,0:T(8,128)(2,1)S(1)} collective-permute-done((bf16[2,128,768]{2,1,0:T(8,128)(2,1)S(1)}, bf16[2,128,768]{2,1,0:T(8,128)(2,1)S(1)}, u32[]{:S(2)}, u32[]{:S(2)}) %collective-permute-start.1) | collective-permute-done | bytes 393248 | tf_op jit(solution)/shard_map/ppermute | solution.py:25
  17.7 0.1 shard_map.168
  17.8 1.9 %collective-permute-start.2 = (bf16[4,128,384]{2,1,0:T(8,128)(2,1)S(1)}, bf16[4,128,384]{2,1,0:T(8,128)(2,1)S(1)}, u32[]{:S(2)}, u32[]{:S(2)}) collective-permute-start(bf16[4,128,384]{2,1,0:T(8,128)(2,1)S(1)} %get-tuple-element.29.both.rest_0_), channel_id=1, source_target_pairs={{4,0},{6,2},{8,4},{10,6},{12,8},{14,10},{0,12},{2,14},{13,1},{15,3... | collective-permute-start | bytes 1179656 | tf_op jit(solution)/shard_map/ppermute | solution.py:25
  19.7 3.4 %collective-permute-start.5 = (bf16[4,128,384]{2,1,0:T(8,128)(2,1)S(1)}, bf16[4,128,384]{2,1,0:T(8,128)(2,1)S(1)}, u32[]{:S(2)}, u32[]{:S(2)}) collective-permute-start(bf16[4,128,384]{2,1,0:T(8,128)(2,1)S(1)} %get-tuple-element.34.both.rest_0_), channel_id=1, source_target_pairs={{4,0},{6,2},{8,4},{10,6},{12,8},{14,10},{0,12},{2,14},{13,1},{15,3... | collective-permute-start | bytes 1179656 | tf_op jit(solution)/shard_map/ppermute | solution.py:25
  23.1 9.6 %collective-permute-done.2.far.rest_1_ = bf16[4,128,384]{2,1,0:T(8,128)(2,1)S(1)} collective-permute-done((bf16[4,128,384]{2,1,0:T(8,128)(2,1)S(1)}, bf16[4,128,384]{2,1,0:T(8,128)(2,1)S(1)}, u32[]{:S(2)}, u32[]{:S(2)}) %collective-permute-start.2) | collective-permute-done | bytes 393248 | tf_op jit(solution)/shard_map/ppermute | solution.py:25
  32.7 0.9 shard_map.169
  33.7 1.9 %collective-permute-start.4 = (bf16[6,128,384]{2,1,0:T(8,128)(2,1)}, bf16[6,128,384]{2,1,0:T(8,128)(2,1)S(1)}, u32[]{:S(2)}, u32[]{:S(2)}) collective-permute-start(bf16[6,128,384]{2,1,0:T(8,128)(2,1)} %get-tuple-element.31), channel_id=1, source_target_pairs={{0,1},{1,0},{2,3},{3,2},{4,5},{5,4},{6,7},{7,6},{8,9},{9,8},{10,11... | collective-permute-start | bytes 1769480 | tf_op jit(solution)/shard_map/ppermute | solution.py:20
  35.6 3.1 %shard_map.166 = (f32[2,32,128]{2,1,0:T(8,128)S(1)}, bf16[2,128,1024]{2,1,0:T(8,128)(2,1)}, bf16[2,128,1024]{2,1,0:T(8,128)(2,1)}, f32[2,2,256]{2,1,0:T(2,128)S(...) custom-call(f32[2,4096]{1,0:T(2,128)} %refs_0_.1, f32[2,4,64]{2,1,0:T(4,128)} %refs_1_.1, ...), custom_call_target="tpu_custom_call" | custom-call | tf_op jit(solution)/shard_map/pallas_call | solution.py:210
  38.7 15.6 %all-to-all-start = ((bf16[32,16,128]{2,1,0:T(8,128)(2,1)}), bf16[32,16,128]{2,1,0:T(8,128)(2,1)S(1)}, u32[]{:S(2)}, u32[]{:S(2)}) async-start(bf16[32,16,128]{2,1,0:T(8,128)(2,1)} %get-tuple-element.22), calls=%async_computation | async-start | bytes 262144 | tf_op jit(solution)/shard_map/all_to_all | solution.py:41
  54.4 0.0 collective-permute-done.5.far.rest_1_
  54.4 0.9 shard_map.171
  55.3 2.1 %collective-permute-start.7 = (bf16[6,128,384]{2,1,0:T(8,128)(2,1)}, bf16[6,128,384]{2,1,0:T(8,128)(2,1)S(1)}, u32[]{:S(2)}, u32[]{:S(2)}) collective-permute-start(bf16[6,128,384]{2,1,0:T(8,128)(2,1)} %get-tuple-element.36), channel_id=1, source_target_pairs={{0,1},{1,0},{2,3},{3,2},{4,5},{5,4},{6,7},{7,6},{8,9},{9,8},{10,11... | collective-permute-start | bytes 1769480 | tf_op jit(solution)/shard_map/ppermute | solution.py:20
  57.4 1.9 %collective-permute-start.3 = (bf16[2,128,384]{2,1,0:T(8,128)(2,1)}, bf16[2,128,384]{2,1,0:T(8,128)(2,1)S(1)}, u32[]{:S(2)}, u32[]{:S(2)}) collective-permute-start(bf16[2,128,384]{2,1,0:T(8,128)(2,1)} %get-tuple-element.30), channel_id=1, source_target_pairs={{2,0},{4,2},{6,4},{8,6},{10,8},{12,10},{14,12},{0,14},{15,1},{1,3}... | collective-permute-start | bytes 589832 | tf_op jit(solution)/shard_map/ppermute | solution.py:25
  59.3 6.1 %all-to-all-done.x = bf16[32,16,128]{2,1,0:T(8,128)(2,1)S(1)} async-done(((bf16[32,16,128]{2,1,0:T(8,128)(2,1)}), bf16[32,16,128]{2,1,0:T(8,128)(2,1)S(1)}, u32[]{:S(2)}, u32[]{:S(2)}) %all-to-all-start) | async-done | bytes 131104 | tf_op jit(solution)/shard_map/all_to_all | solution.py:41
  65.4 1.0 collective-permute-done.3.rest_2_
  66.4 0.0 collective-permute-done.4.rest_3_
  66.4 1.9 %mixer_step.2 = (bf16[32,8,128]{2,1,0:T(8,128)(2,1)S(1)}, f32[16,512]{1,0:T(8,128)S(1)}) custom-call(s32[1]{0:T(128)} %bitcast.here, bf16[32,16,128]{2,1,0:T(8,128)(2,1)S(1)} %all-to-all-done.x, f32[2,32,128]{2,1,0:T(8,128)S(1)} %get-tuple-element.23.gain, bf16[2,128,1024]{2,1,0:T(8,128)(2,1)} %get-tuple-element.24.drive_far, ...), custom_call_target="tpu_custom_call" | custom-call | tf_op jit(solution)/shard_map/mixer_step/pallas_call | solution.py:227
  68.3 0.0 copy-start
  68.4 19.3 %all_to_all.20.mixed = bf16[32,8,128]{2,1,0:T(8,128)(2,1)S(1)} all-to-all(bf16[32,8,128]{2,1,0:T(8,128)(2,1)S(1)} %get-tuple-element.32), channel_id=1, replica_groups=mesh['tp'=32,'dp'=16] {'tp'}, dimensions={0} | all-to-all | bytes 131072 | tf_op jit(solution)/shard_map/all_to_all | solution.py:41
  87.7 0.0 copy-done
  87.7 1.0 shard_map.170
  88.7 3.9 %all-to-all-start.2 = ((bf16[32,16,128]{2,1,0:T(8,128)(2,1)}), bf16[32,16,128]{2,1,0:T(8,128)(2,1)S(1)}, u32[]{:S(2)}, u32[]{:S(2)}) async-start(bf16[32,16,128]{2,1,0:T(8,128)(2,1)} %get-tuple-element.33), calls=%async_computation.2 | async-start | bytes 262144 | tf_op jit(solution)/shard_map/all_to_all | solution.py:41
  92.5 1.9 %collective-permute-start.6 = (bf16[2,128,384]{2,1,0:T(8,128)(2,1)S(1)}, bf16[2,128,384]{2,1,0:T(8,128)(2,1)S(1)}, u32[]{:S(2)}, u32[]{:S(2)}) collective-permute-start(bf16[2,128,384]{2,1,0:T(8,128)(2,1)S(1)} %get-tuple-element.35), channel_id=1, source_target_pairs={{2,0},{4,2},{6,4},{8,6},{10,8},{12,10},{14,12},{0,14},{15,1},{1,3}... | collective-permute-start | bytes 589832 | tf_op jit(solution)/shard_map/ppermute | solution.py:25
  94.4 6.8 %collective-permute-done.6.rest_2_ = bf16[2,128,384]{2,1,0:T(8,128)(2,1)S(1)} collective-permute-done((bf16[2,128,384]{2,1,0:T(8,128)(2,1)S(1)}, bf16[2,128,384]{2,1,0:T(8,128)(2,1)S(1)}, u32[]{:S(2)}, u32[]{:S(2)}) %collective-permute-start.6) | collective-permute-done | bytes 196640 | tf_op jit(solution)/shard_map/ppermute | solution.py:25
  101.3 0.0 collective-permute-done.7.rest_3_
  101.3 1.8 %all-to-all-done.2.x = bf16[32,16,128]{2,1,0:T(8,128)(2,1)S(1)} async-done(((bf16[32,16,128]{2,1,0:T(8,128)(2,1)}), bf16[32,16,128]{2,1,0:T(8,128)(2,1)S(1)}, u32[]{:S(2)}, u32[]{:S(2)}) %all-to-all-start.2) | async-done | bytes 131104 | tf_op jit(solution)/shard_map/all_to_all | solution.py:41
  103.1 1.6 %mixer_step.3 = (bf16[32,8,128]{2,1,0:T(8,128)(2,1)S(1)}, f32[16,512]{1,0:T(8,128)S(1)}) custom-call(s32[1]{0:T(128)} %bitcast.here, bf16[32,16,128]{2,1,0:T(8,128)(2,1)S(1)} %all-to-all-done.2.x, f32[2,32,128]{2,1,0:T(8,128)S(1)} %get-tuple-element.23.gain, bf16[2,128,1024]{2,1,0:T(8,128)(2,1)} %get-tuple-element.24.drive_far, ...), custom_call_target="tpu_custom_call" | custom-call | tf_op jit(solution)/shard_map/mixer_step/pallas_call | solution.py:227
  104.7 17.8 %all_to_all.21.mixed = bf16[32,8,128]{2,1,0:T(8,128)(2,1)S(1)} all-to-all(bf16[32,8,128]{2,1,0:T(8,128)(2,1)S(1)} %get-tuple-element.37), channel_id=1, replica_groups=mesh['tp'=32,'dp'=16] {'tp'}, dimensions={0} | all-to-all | bytes 131072 | tf_op jit(solution)/shard_map/all_to_all | solution.py:41
  122.5 0.9 shard_map.172
  (1 shorter events, 0.0 us)
Async XLA Ops:
  1.6 3.3 %collective-permute-start = (bf16[1,128,768]{2,1,0:T(8,128)(2,1)S(1)}, bf16[1,128,768]{2,1,0:T(8,128)(2,1)S(1)}, u32[]{:S(2)}, u32[]{:S(2)}) collective-permute-start(bf16[1,128,768]{2,1,0:T(8,128)(2,1)S(1)} %shard_map.167), channel_id=1, source_target_pairs={{0,1},{1,0},{2,3},{3,2},{4,5},{5,4},{6,7},{7,6},{8,9},{9,8},{10,11... | collective-permute-start | bytes 589832 | tf_op jit(solution)/shard_map/ppermute | solution.py:20
  5.0 12.8 %collective-permute-start.1 = (bf16[2,128,768]{2,1,0:T(8,128)(2,1)S(1)}, bf16[2,128,768]{2,1,0:T(8,128)(2,1)S(1)}, u32[]{:S(2)}, u32[]{:S(2)}) collective-permute-start(bf16[2,128,768]{2,1,0:T(8,128)(2,1)S(1)} %pad_maximum_fusion.pair), channel_id=1, source_target_pairs={{2,0},{4,2},{6,4},{8,6},{10,8},{12,10},{14,12},{0,14},{15,1},{1,3}... | collective-permute-start | bytes 1179656 | tf_op jit(solution)/shard_map/ppermute | solution.py:25
  17.8 14.9 %collective-permute-start.2 = (bf16[4,128,384]{2,1,0:T(8,128)(2,1)S(1)}, bf16[4,128,384]{2,1,0:T(8,128)(2,1)S(1)}, u32[]{:S(2)}, u32[]{:S(2)}) collective-permute-start(bf16[4,128,384]{2,1,0:T(8,128)(2,1)S(1)} %get-tuple-element.29.both.rest_0_), channel_id=1, source_target_pairs={{4,0},{6,2},{8,4},{10,6},{12,8},{14,10},{0,12},{2,14},{13,1},{15,3... | collective-permute-start | bytes 1179656 | tf_op jit(solution)/shard_map/ppermute | solution.py:25
  19.7 34.6 %collective-permute-start.5 = (bf16[4,128,384]{2,1,0:T(8,128)(2,1)S(1)}, bf16[4,128,384]{2,1,0:T(8,128)(2,1)S(1)}, u32[]{:S(2)}, u32[]{:S(2)}) collective-permute-start(bf16[4,128,384]{2,1,0:T(8,128)(2,1)S(1)} %get-tuple-element.34.both.rest_0_), channel_id=1, source_target_pairs={{4,0},{6,2},{8,4},{10,6},{12,8},{14,10},{0,12},{2,14},{13,1},{15,3... | collective-permute-start | bytes 1179656 | tf_op jit(solution)/shard_map/ppermute | solution.py:25
  33.7 32.7 %collective-permute-start.4 = (bf16[6,128,384]{2,1,0:T(8,128)(2,1)}, bf16[6,128,384]{2,1,0:T(8,128)(2,1)S(1)}, u32[]{:S(2)}, u32[]{:S(2)}) collective-permute-start(bf16[6,128,384]{2,1,0:T(8,128)(2,1)} %get-tuple-element.31), channel_id=1, source_target_pairs={{0,1},{1,0},{2,3},{3,2},{4,5},{5,4},{6,7},{7,6},{8,9},{9,8},{10,11... | collective-permute-start | bytes 1769480 | tf_op jit(solution)/shard_map/ppermute | solution.py:20
  38.7 26.7 %all-to-all-start = ((bf16[32,16,128]{2,1,0:T(8,128)(2,1)}), bf16[32,16,128]{2,1,0:T(8,128)(2,1)S(1)}, u32[]{:S(2)}, u32[]{:S(2)}) async-start(bf16[32,16,128]{2,1,0:T(8,128)(2,1)} %get-tuple-element.22), calls=%async_computation | async-start | bytes 262144 | tf_op jit(solution)/shard_map/all_to_all | solution.py:41
  55.3 46.0 %collective-permute-start.7 = (bf16[6,128,384]{2,1,0:T(8,128)(2,1)}, bf16[6,128,384]{2,1,0:T(8,128)(2,1)S(1)}, u32[]{:S(2)}, u32[]{:S(2)}) collective-permute-start(bf16[6,128,384]{2,1,0:T(8,128)(2,1)} %get-tuple-element.36), channel_id=1, source_target_pairs={{0,1},{1,0},{2,3},{3,2},{4,5},{5,4},{6,7},{7,6},{8,9},{9,8},{10,11... | collective-permute-start | bytes 1769480 | tf_op jit(solution)/shard_map/ppermute | solution.py:20
  57.4 9.0 %collective-permute-start.3 = (bf16[2,128,384]{2,1,0:T(8,128)(2,1)}, bf16[2,128,384]{2,1,0:T(8,128)(2,1)S(1)}, u32[]{:S(2)}, u32[]{:S(2)}) collective-permute-start(bf16[2,128,384]{2,1,0:T(8,128)(2,1)} %get-tuple-element.30), channel_id=1, source_target_pairs={{2,0},{4,2},{6,4},{8,6},{10,8},{12,10},{14,12},{0,14},{15,1},{1,3}... | collective-permute-start | bytes 589832 | tf_op jit(solution)/shard_map/ppermute | solution.py:25
  68.3 19.3 %copy-start = (bf16[16,128]{1,0:T(8,128)(2,1)S(1)}, bf16[16,128]{1,0:T(8,128)(2,1)}, u32[]{:S(2)}) copy-start(bf16[16,128]{1,0:T(8,128)(2,1)} %before.1) | copy-start | bytes 12292
  88.7 14.4 %all-to-all-start.2 = ((bf16[32,16,128]{2,1,0:T(8,128)(2,1)}), bf16[32,16,128]{2,1,0:T(8,128)(2,1)S(1)}, u32[]{:S(2)}, u32[]{:S(2)}) async-start(bf16[32,16,128]{2,1,0:T(8,128)(2,1)} %get-tuple-element.33), calls=%async_computation.2 | async-start | bytes 262144 | tf_op jit(solution)/shard_map/all_to_all | solution.py:41
  92.5 8.8 %collective-permute-start.6 = (bf16[2,128,384]{2,1,0:T(8,128)(2,1)S(1)}, bf16[2,128,384]{2,1,0:T(8,128)(2,1)S(1)}, u32[]{:S(2)}, u32[]{:S(2)}) collective-permute-start(bf16[2,128,384]{2,1,0:T(8,128)(2,1)S(1)} %get-tuple-element.35), channel_id=1, source_target_pairs={{2,0},{4,2},{6,4},{8,6},{10,8},{12,10},{14,12},{0,14},{15,1},{1,3}... | collective-permute-start | bytes 589832 | tf_op jit(solution)/shard_map/ppermute | solution.py:25

commit v3 on v2

--- a/solution.py
+++ b/solution.py
@@ -14,6 +14,7 @@
 
 
 PARTNER = [(i, i ^ 1) for i in range(16)]
+DIAGONAL = [(2 * ((y + 1) % 8) + 1, 2 * y) for y in range(8)] + [(2 * ((y - 1) % 8), 2 * y + 1) for y in range(8)]
 
 
 def to_partner(array):
@@ -27,13 +28,11 @@
 
 def shards_of(here, pieces):
     y, c = here >> 1, here & 1
-    way = 1 - 2 * c
-    order = [(0, 0, 0), (0, 2, 1), (1, 0, 2), (1, 2, 3), (2, 0, 4), (3, 0, -1), (3, 2, -2), (3, 4, -3)]
     found = []
-    for array, at, k in order:
-        first = c if array < 3 else 1 - c
-        base = 2 * ((y + way * k) & 7)
-        found += [(base + first, pieces[array], at), (base + 1 - first, pieces[array], at + 1)]
+    for array, core in ((pieces[0], c), (pieces[1], 1 - c)):
+        for i in range(8):
+            side = core if i % 2 == 0 else 1 - core
+            found.append((2 * ((y + (1 - 2 * core) * ((i + 1) // 2)) & 7) + side, array, i))
     return found
 
 
@@ -55,6 +54,10 @@
     return body
 
 
+def copy_kernel(tokens, copies):
+    copies[...] = jnp.broadcast_to(tokens[...][None], copies.shape)
+
+
 def send_kernel(w_in, w_gate, w_out, shard):
     for l in range(2):
         at = 384 * l
@@ -64,8 +67,7 @@
 
 
 def stack_kernel(pair, near, both0, both1):
-    for l, both in ((0, both0), (1, both1)):
-        lanes = slice(384 * l, 384 * l + 384)
+    for both, lanes in ((both0, slice(0, 256)), (both1, slice(256, 768))):
         both[0:2] = pair[:, :, lanes]
         both[2:4] = near[:, :, lanes]
 
@@ -75,14 +77,12 @@
     return upper, (array - upper.astype(F32)).astype(BF16)
 
 
-def join_kernel(both, far, joined, last):
-    joined[0:2] = both[2:4]
-    joined[2:6] = far[...]
-    last[...] = far[2:4]
-
-
-def prepare_kernel(gains, decay_rate, frequency, log_step, map_re, map_im, read_re, read_im, skip_weight, state_re, state_im, tokens, gain, drive_far, read_far, decay, skip, old, copies, drive, read, drive_parts, read_parts, sems):
-    copies[...] = jnp.broadcast_to(tokens[...][None], copies.shape)
+def join_kernel(both, far, joined):
+    joined[0:4] = both[...]
+    joined[4:8] = far[...]
+
+
+def prepare_kernel(gains, decay_rate, frequency, log_step, map_re, map_im, read_re, read_im, skip_weight, state_re, state_im, gain, drive_far, read_far, decay, skip, old, drive, read, drive_parts, read_parts, sems):
     drive[...] = jnp.zeros(drive.shape, F32)
     read[...] = jnp.zeros(read.shape, F32)
     skip[...] = jnp.zeros(skip.shape, F32)
@@ -139,7 +139,7 @@
         left = (x[t].astype(F32) * inv_scale * gain[layer, pl.ds(t, 1), :]).astype(BF16)
         right = (x[t + 1].astype(F32) * inv_scale * gain[layer, pl.ds(t + 1, 1), :]).astype(BF16)
         rows = jnp.concatenate([left, right], axis=1)
-        turned += lax.dot_general(array[at, :, 0:256], rows, (((1,), (1,)), ((), ())), preferred_element_type=F32)
+        turned += lax.dot_general(array[at, :, 128 * layer : 128 * layer + 256], rows, (((1,), (1,)), ((), ())), preferred_element_type=F32)
     both = turned.T.astype(BF16).astype(F32)
     get_drive.wait()
     parts = jnp.dot(both.astype(BF16), drive[...], preferred_element_type=F32)
@@ -163,7 +163,7 @@
 
 
 def out_kernel(layer, here, mixed, before, *rest):
-    pieces, outs = rest[:4], rest[4:]
+    pieces, outs = rest[:2], rest[2:]
     low = lax.broadcasted_iota(jnp.int32, (8, 128), 1) < 64
     total = jnp.zeros((16, 128), F32)
     for block, array, at in shards_of(here[0], pieces):
@@ -173,7 +173,7 @@
         upper = jnp.where(low, a, pltpu.roll(b, 64, axis=1))
         lower = jnp.where(low, pltpu.roll(a, 64, axis=1), b)
         rows = jnp.concatenate([upper, lower], axis=0).astype(BF16)
-        total += jnp.dot(rows, array[at, :, 256:384], preferred_element_type=F32)
+        total += jnp.dot(rows, array[at, :, 384 * layer : 384 * layer + 128], preferred_element_type=F32)
     hidden = (before[...].astype(F32) + total).astype(BF16)
     if layer == 0:
         outs[0][...] = hidden
@@ -240,25 +240,24 @@
     shard = run_loaded(
         send_kernel, (w_in.transpose(0, 2, 1), w_gate.transpose(0, 2, 1), w_out), [((1, 128, 768), BF16)], (0,)
     )[0]
-    *small, copies = run_loaded(
+    small = run_loaded(
         prepare_kernel,
-        (norm_gain, decay_rate, frequency, log_step, map_re, map_im, read_re, read_im, skip_weight, state_re, state_im, tokens),
-        [((2, 32, 128), F32), ((2, 128, 1024), BF16), ((2, 128, 1024), BF16), ((2, 2, 256), F32), ((2, 1, 128), F32), ((2, 2, 16, 256), F32), ((32, 16, 128), BF16)],
+        (norm_gain, decay_rate, frequency, log_step, map_re, map_im, read_re, read_im, skip_weight, state_re, state_im),
+        [((2, 32, 128), F32), ((2, 128, 1024), BF16), ((2, 128, 1024), BF16), ((2, 2, 256), F32), ((2, 1, 128), F32), ((2, 2, 16, 256), F32)],
         (0, 3, 4, 5),
         (1, 2),
         [pltpu.VMEM((2, 128, 512), F32)] * 2 + [pltpu.VMEM((2, 128, 1024), BF16)] * 2 + [pltpu.SemaphoreType.DMA((2,))],
     )
-    pair = jnp.concatenate([shard, to_partner(shard)])
+    copies = run_loaded(copy_kernel, (tokens,), [((32, 16, 128), BF16)])[0]
+    pair = jnp.concatenate([shard, lax.ppermute(shard, "dp", DIAGONAL)])
     near = from_y(pair, 1)
-    both0, both1 = run(stack_kernel, close(pair, near), [((4, 128, 384), BF16)] * 2, range(2))
+    both0, both1 = run(stack_kernel, close(pair, near), [((4, 128, 256), BF16), ((4, 128, 512), BF16)], range(2))
 
     def pieces_of(both):
         far = from_y(both, 2)
-        shapes = [((6, 128, 384), BF16), ((2, 128, 384), BF16)]
-        joined, last = run(join_kernel, close(both, far), shapes, (0, 1))
-        last = from_y(last, 1)
+        joined = run(join_kernel, close(both, far), [((8, 128, both.shape[2]), BF16)], (0,))[0]
         across = to_partner(joined)
-        return [both, far, last, across]
+        return [joined, across]
 
     gathered = over_tp(copies)
     first = pieces_of(both0)
@@ -266,7 +265,7 @@
     second = pieces_of(both1)
     mixed = over_tp(mixed)
     shapes = [((16, 128), BF16), ((32, 16, 128), BF16)]
-    hidden, copies = run(functools.partial(out_kernel, 0), (here, *close(mixed), tokens, *close(*first)), shapes, (0,), 1)
+    hidden, copies = run(functools.partial(out_kernel, 0), (here, *close(mixed), tokens, *close(*second)), shapes, (0,), 1)
     gathered = over_tp(copies)
     mixed, fresh1 = mixer_call(1, here, gathered, small, second)
     shapes = [((16, 128), BF16), (state_re.shape, F32), (state_im.shape, F32)]

time: 124 us -> 125 us (level)
  the two profiles are of different devices: /device:TPU:56 before, /device:TPU:24 now
where the time goes in v3:
time: 125 us
  waiting for transfers between devices  45.3 us (36%)
  blocking collectives  40.2 us (32%)
  starting transfers between devices  28.8 us (23%)
  Pallas kernels  9.75 us (8%)
    all_to_all x3, blocking collectives, over_tp(): return lax.all_to_all(copies, 'tp', split_axis=0, concat_axis=0, tiled=True)  40.2 us
    ppermute x3, waiting for transfers between devices, from_y(): return lax.ppermute(array, 'dp', pairs)  32.7 us
    all_to_all x1, starting transfers between devices, over_tp(): return lax.all_to_all(copies, 'tp', split_axis=0, concat_axis=0, tiled=True)  12.8 us
    all_to_all x1, waiting for transfers between devices, over_tp(): return lax.all_to_all(copies, 'tp', split_axis=0, concat_axis=0, tiled=True)  8.57 us
    ppermute x3, starting transfers between devices, from_y(): return lax.ppermute(array, 'dp', pairs)  7.96 us
    pallas_call x3, Pallas kernels, run_loaded(): pl.pallas_call(loaded(kernel, len(args), len(shapes)), in_specs=[pl.Block...  4.79 us
    ppermute x1, starting transfers between devices, local(): pair = jnp.concatenate([shard, lax.ppermute(shard, 'dp', DIAGONAL)])  4.13 us
    ppermute x1, waiting for transfers between devices, local(): pair = jnp.concatenate([shard, lax.ppermute(shard, 'dp', DIAGONAL)])  4.06 us
  transfers between devices with their start and end apart: 7, of which 5 were waited for; matrix products, arithmetic and copies ran while one was open for 0% of the time, Pallas kernels for 5%

profile of v3, /device:TPU:24, one launch (start us, length us, event | category | flops | bytes accessed | tf_op | source)
XLA Modules:
  0.0 124.8 jit_solution(13440113147525180418)
XLA Ops:
  0.6 0.9 shard_map.168
  1.6 4.1 %collective-permute-start = (bf16[1,128,768]{2,1,0:T(8,128)(2,1)S(1)}, bf16[1,128,768]{2,1,0:T(8,128)(2,1)S(1)}, u32[]{:S(2)}, u32[]{:S(2)}) collective-permute-start(bf16[1,128,768]{2,1,0:T(8,128)(2,1)S(1)} %shard_map.168), channel_id=1, source_target_pairs={{3,0},{5,2},{7,4},{9,6},{11,8},{13,10},{15,12},{1,14},{14,1},{0,3}... | collective-permute-start | bytes 589832 | tf_op jit(solution)/shard_map/ppermute | solution.py:252
  5.7 4.1 %collective-permute-done = bf16[1,128,768]{2,1,0:T(8,128)(2,1)S(1)} collective-permute-done((bf16[1,128,768]{2,1,0:T(8,128)(2,1)S(1)}, bf16[1,128,768]{2,1,0:T(8,128)(2,1)S(1)}, u32[]{:S(2)}, u32[]{:S(2)}) %collective-permute-start) | collective-permute-done | bytes 196640 | tf_op jit(solution)/shard_map/ppermute | solution.py:252
  9.8 1.9 %collective-permute-start.1 = (bf16[2,128,768]{2,1,0:T(8,128)(2,1)S(1)}, bf16[2,128,768]{2,1,0:T(8,128)(2,1)S(1)}, u32[]{:S(2)}, u32[]{:S(2)}) collective-permute-start(bf16[2,128,768]{2,1,0:T(8,128)(2,1)S(1)} %pad_maximum_fusion.pair), channel_id=1, source_target_pairs={{2,0},{4,2},{6,4},{8,6},{10,8},{12,10},{14,12},{0,14},{15,1},{1,3}... | collective-permute-start | bytes 1179656 | tf_op jit(solution)/shard_map/ppermute | solution.py:26
  11.8 9.0 %collective-permute-done.1.near = bf16[2,128,768]{2,1,0:T(8,128)(2,1)S(1)} collective-permute-done((bf16[2,128,768]{2,1,0:T(8,128)(2,1)S(1)}, bf16[2,128,768]{2,1,0:T(8,128)(2,1)S(1)}, u32[]{:S(2)}, u32[]{:S(2)}) %collective-permute-start.1) | collective-permute-done | bytes 393248 | tf_op jit(solution)/shard_map/ppermute | solution.py:26
  20.7 0.1 shard_map.169
  20.8 3.1 %collective-permute-start.4 = (bf16[4,128,512]{2,1,0:T(8,128)(2,1)S(1)}, bf16[4,128,512]{2,1,0:T(8,128)(2,1)S(1)}, u32[]{:S(2)}, u32[]{:S(2)}) collective-permute-start(bf16[4,128,512]{2,1,0:T(8,128)(2,1)S(1)} %get-tuple-element.25.both), channel_id=1, source_target_pairs={{4,0},{6,2},{8,4},{10,6},{12,8},{14,10},{0,12},{2,14},{13,1},{15,3... | collective-permute-start | bytes 1572872 | tf_op jit(solution)/shard_map/ppermute | solution.py:26
  23.9 14.5 %collective-permute-done.4.far = bf16[4,128,512]{2,1,0:T(8,128)(2,1)S(1)} collective-permute-done((bf16[4,128,512]{2,1,0:T(8,128)(2,1)S(1)}, bf16[4,128,512]{2,1,0:T(8,128)(2,1)S(1)}, u32[]{:S(2)}, u32[]{:S(2)}) %collective-permute-start.4) | collective-permute-done | bytes 524320 | tf_op jit(solution)/shard_map/ppermute | solution.py:26
  38.4 0.1 shard_map.171.rest_0_
  38.5 1.9 %collective-permute-start.5 = (bf16[8,128,512]{2,1,0:T(8,128)(2,1)S(1)}, bf16[8,128,512]{2,1,0:T(8,128)(2,1)S(1)}, u32[]{:S(2)}, u32[]{:S(2)}) collective-permute-start(bf16[8,128,512]{2,1,0:T(8,128)(2,1)S(1)} %shard_map.171.rest_0_), channel_id=1, source_target_pairs={{0,1},{1,0},{2,3},{3,2},{4,5},{5,4},{6,7},{7,6},{8,9},{9,8},{10,11... | collective-permute-start | bytes 3145736 | tf_op jit(solution)/shard_map/ppermute | solution.py:21
  40.4 2.9 %collective-permute-start.2 = (bf16[4,128,256]{2,1,0:T(8,128)(2,1)S(1)}, bf16[4,128,256]{2,1,0:T(8,128)(2,1)S(1)}, u32[]{:S(2)}, u32[]{:S(2)}) collective-permute-start(bf16[4,128,256]{2,1,0:T(8,128)(2,1)S(1)} %get-tuple-element.23.both), channel_id=1, source_target_pairs={{4,0},{6,2},{8,4},{10,6},{12,8},{14,10},{0,12},{2,14},{13,1},{15,3... | collective-permute-start | bytes 786440 | tf_op jit(solution)/shard_map/ppermute | solution.py:26
  43.3 9.3 %collective-permute-done.2.far = bf16[4,128,256]{2,1,0:T(8,128)(2,1)S(1)} collective-permute-done((bf16[4,128,256]{2,1,0:T(8,128)(2,1)S(1)}, bf16[4,128,256]{2,1,0:T(8,128)(2,1)S(1)}, u32[]{:S(2)}, u32[]{:S(2)}) %collective-permute-start.2) | collective-permute-done | bytes 262176 | tf_op jit(solution)/shard_map/ppermute | solution.py:26
  52.6 1.9 %collective-permute-start.3 = (bf16[8,128,256]{2,1,0:T(8,128)(2,1)S(1)}, bf16[8,128,256]{2,1,0:T(8,128)(2,1)S(1)}, u32[]{:S(2)}, u32[]{:S(2)}) collective-permute-start(bf16[8,128,256]{2,1,0:T(8,128)(2,1)S(1)} %shard_map.170.rest_0_), channel_id=1, source_target_pairs={{0,1},{1,0},{2,3},{3,2},{4,5},{5,4},{6,7},{7,6},{8,9},{9,8},{10,11... | collective-permute-start | bytes 1572872 | tf_op jit(solution)/shard_map/ppermute | solution.py:21
  54.6 1.4 %shard_map.166 = bf16[32,16,128]{2,1,0:T(8,128)(2,1)} custom-call(bf16[16,128]{1,0:T(8,128)(2,1)} %before.1), custom_call_target="tpu_custom_call" | custom-call | tf_op jit(solution)/shard_map/pallas_call | solution.py:210
  55.9 12.8 %all-to-all-start = ((bf16[32,16,128]{2,1,0:T(8,128)(2,1)}), bf16[32,16,128]{2,1,0:T(8,128)(2,1)S(1)}, u32[]{:S(2)}, u32[]{:S(2)}) async-start(bf16[32,16,128]{2,1,0:T(8,128)(2,1)} %shard_map.166), calls=%async_computation | async-start | bytes 262144 | tf_op jit(solution)/shard_map/all_to_all | solution.py:40
  68.7 2.5 %shard_map.167 = (f32[2,32,128]{2,1,0:T(8,128)S(1)}, bf16[2,128,1024]{2,1,0:T(8,128)(2,1)}, bf16[2,128,1024]{2,1,0:T(8,128)(2,1)}, f32[2,2,256]{2,1,0:T(2,128)S(...) custom-call(f32[2,4096]{1,0:T(2,128)} %refs_0_.3, f32[2,4,64]{2,1,0:T(4,128)} %refs_1_.1, ...), custom_call_target="tpu_custom_call" | custom-call | tf_op jit(solution)/shard_map/pallas_call | solution.py:210
  71.2 8.6 %all-to-all-done.x = bf16[32,16,128]{2,1,0:T(8,128)(2,1)S(1)} async-done(((bf16[32,16,128]{2,1,0:T(8,128)(2,1)}), bf16[32,16,128]{2,1,0:T(8,128)(2,1)S(1)}, u32[]{:S(2)}, u32[]{:S(2)}) %all-to-all-start) | async-done | bytes 131104 | tf_op jit(solution)/shard_map/all_to_all | solution.py:40
  79.8 0.0 collective-permute-done.3.rest_1_
  79.8 1.9 %mixer_step.2 = (bf16[32,8,128]{2,1,0:T(8,128)(2,1)S(1)}, f32[16,512]{1,0:T(8,128)S(1)}) custom-call(s32[1]{0:T(128)} %bitcast.here, bf16[32,16,128]{2,1,0:T(8,128)(2,1)S(1)} %all-to-all-done.x, f32[2,32,128]{2,1,0:T(8,128)S(1)} %get-tuple-element.17.gain, bf16[2,128,1024]{2,1,0:T(8,128)(2,1)} %get-tuple-element.18.drive_far, ...), custom_call_target="tpu_custom_call" | custom-call | tf_op jit(solution)/shard_map/mixer_step/pallas_call | solution.py:227
  81.8 0.0 copy-start
  81.8 13.4 %all_to_all.20.mixed = bf16[32,8,128]{2,1,0:T(8,128)(2,1)S(1)} all-to-all(bf16[32,8,128]{2,1,0:T(8,128)(2,1)S(1)} %get-tuple-element.24), channel_id=1, replica_groups=mesh['tp'=32,'dp'=16] {'tp'}, dimensions={0} | all-to-all | bytes 131072 | tf_op jit(solution)/shard_map/all_to_all | solution.py:40
  95.1 0.0 collective-permute-done.5.rest_1_
  95.1 0.0 copy-done
  95.1 0.3 shard_map.172
  95.5 13.7 %all_to_all.21.x = bf16[32,16,128]{2,1,0:T(8,128)(2,1)S(1)} all-to-all(bf16[32,16,128]{2,1,0:T(8,128)(2,1)S(1)} %get-tuple-element.26), channel_id=1, replica_groups=mesh['tp'=32,'dp'=16] {'tp'}, dimensions={0} | all-to-all | bytes 262144 | tf_op jit(solution)/shard_map/all_to_all | solution.py:40
  109.2 1.6 %mixer_step.3 = (bf16[32,8,128]{2,1,0:T(8,128)(2,1)S(1)}, f32[16,512]{1,0:T(8,128)S(1)}) custom-call(s32[1]{0:T(128)} %bitcast.here, bf16[32,16,128]{2,1,0:T(8,128)(2,1)S(1)} %all_to_all.21.x, f32[2,32,128]{2,1,0:T(8,128)S(1)} %get-tuple-element.17.gain, bf16[2,128,1024]{2,1,0:T(8,128)(2,1)} %get-tuple-element.18.drive_far, ...), custom_call_target="tpu_custom_call" | custom-call | tf_op jit(solution)/shard_map/mixer_step/pallas_call | solution.py:227
  110.8 13.1 %all_to_all.22.mixed = bf16[32,8,128]{2,1,0:T(8,128)(2,1)S(1)} all-to-all(bf16[32,8,128]{2,1,0:T(8,128)(2,1)S(1)} %get-tuple-element.27), channel_id=1, replica_groups=mesh['tp'=32,'dp'=16] {'tp'}, dimensions={0} | all-to-all | bytes 131072 | tf_op jit(solution)/shard_map/all_to_all | solution.py:40
  123.9 0.9 shard_map.173
  (2 shorter events, 0.1 us)
Async XLA Ops:
  1.6 8.2 %collective-permute-start = (bf16[1,128,768]{2,1,0:T(8,128)(2,1)S(1)}, bf16[1,128,768]{2,1,0:T(8,128)(2,1)S(1)}, u32[]{:S(2)}, u32[]{:S(2)}) collective-permute-start(bf16[1,128,768]{2,1,0:T(8,128)(2,1)S(1)} %shard_map.168), channel_id=1, source_target_pairs={{3,0},{5,2},{7,4},{9,6},{11,8},{13,10},{15,12},{1,14},{14,1},{0,3}... | collective-permute-start | bytes 589832 | tf_op jit(solution)/shard_map/ppermute | solution.py:252
  9.8 10.9 %collective-permute-start.1 = (bf16[2,128,768]{2,1,0:T(8,128)(2,1)S(1)}, bf16[2,128,768]{2,1,0:T(8,128)(2,1)S(1)}, u32[]{:S(2)}, u32[]{:S(2)}) collective-permute-start(bf16[2,128,768]{2,1,0:T(8,128)(2,1)S(1)} %pad_maximum_fusion.pair), channel_id=1, source_target_pairs={{2,0},{4,2},{6,4},{8,6},{10,8},{12,10},{14,12},{0,14},{15,1},{1,3}... | collective-permute-start | bytes 1179656 | tf_op jit(solution)/shard_map/ppermute | solution.py:26
  20.8 17.7 %collective-permute-start.4 = (bf16[4,128,512]{2,1,0:T(8,128)(2,1)S(1)}, bf16[4,128,512]{2,1,0:T(8,128)(2,1)S(1)}, u32[]{:S(2)}, u32[]{:S(2)}) collective-permute-start(bf16[4,128,512]{2,1,0:T(8,128)(2,1)S(1)} %get-tuple-element.25.both), channel_id=1, source_target_pairs={{4,0},{6,2},{8,4},{10,6},{12,8},{14,10},{0,12},{2,14},{13,1},{15,3... | collective-permute-start | bytes 1572872 | tf_op jit(solution)/shard_map/ppermute | solution.py:26
  38.5 56.6 %collective-permute-start.5 = (bf16[8,128,512]{2,1,0:T(8,128)(2,1)S(1)}, bf16[8,128,512]{2,1,0:T(8,128)(2,1)S(1)}, u32[]{:S(2)}, u32[]{:S(2)}) collective-permute-start(bf16[8,128,512]{2,1,0:T(8,128)(2,1)S(1)} %shard_map.171.rest_0_), channel_id=1, source_target_pairs={{0,1},{1,0},{2,3},{3,2},{4,5},{5,4},{6,7},{7,6},{8,9},{9,8},{10,11... | collective-permute-start | bytes 3145736 | tf_op jit(solution)/shard_map/ppermute | solution.py:21
  40.4 12.2 %collective-permute-start.2 = (bf16[4,128,256]{2,1,0:T(8,128)(2,1)S(1)}, bf16[4,128,256]{2,1,0:T(8,128)(2,1)S(1)}, u32[]{:S(2)}, u32[]{:S(2)}) collective-permute-start(bf16[4,128,256]{2,1,0:T(8,128)(2,1)S(1)} %get-tuple-element.23.both), channel_id=1, source_target_pairs={{4,0},{6,2},{8,4},{10,6},{12,8},{14,10},{0,12},{2,14},{13,1},{15,3... | collective-permute-start | bytes 786440 | tf_op jit(solution)/shard_map/ppermute | solution.py:26
  52.6 27.2 %collective-permute-start.3 = (bf16[8,128,256]{2,1,0:T(8,128)(2,1)S(1)}, bf16[8,128,256]{2,1,0:T(8,128)(2,1)S(1)}, u32[]{:S(2)}, u32[]{:S(2)}) collective-permute-start(bf16[8,128,256]{2,1,0:T(8,128)(2,1)S(1)} %shard_map.170.rest_0_), channel_id=1, source_target_pairs={{0,1},{1,0},{2,3},{3,2},{4,5},{5,4},{6,7},{7,6},{8,9},{9,8},{10,11... | collective-permute-start | bytes 1572872 | tf_op jit(solution)/shard_map/ppermute | solution.py:21
  55.9 23.9 %all-to-all-start = ((bf16[32,16,128]{2,1,0:T(8,128)(2,1)}), bf16[32,16,128]{2,1,0:T(8,128)(2,1)S(1)}, u32[]{:S(2)}, u32[]{:S(2)}) async-start(bf16[32,16,128]{2,1,0:T(8,128)(2,1)} %shard_map.166), calls=%async_computation | async-start | bytes 262144 | tf_op jit(solution)/shard_map/all_to_all | solution.py:40
  81.8 13.4 %copy-start = (bf16[16,128]{1,0:T(8,128)(2,1)S(1)}, bf16[16,128]{1,0:T(8,128)(2,1)}, u32[]{:S(2)}) copy-start(bf16[16,128]{1,0:T(8,128)(2,1)} %before.1) | copy-start | bytes 12292

commit v4 on v3

--- a/solution.py
+++ b/solution.py
@@ -124,24 +124,50 @@
         move.wait()
 
 
-def mixer_kernel(layer, here, x, gain, drive_far, read_far, decay, skip, old, *rest):
-    pieces, (mixed, fresh_out, drive, read, sems) = rest[:-5], rest[-5:]
-    get_drive = pltpu.make_async_copy(drive_far.at[layer], drive, sems.at[0])
-    get_read = pltpu.make_async_copy(read_far.at[layer], read, sems.at[1])
-    get_drive.start()
-    get_read.start()
+def scale_of(x):
     wide = x[...].astype(F32)
     square = jnp.sum(jnp.sum(wide * wide, axis=0), axis=1, keepdims=True)
-    inv_scale = lax.rsqrt(square * (1.0 / 4096) + EPSILON)
-    turned = jnp.zeros((128, 16), F32)
-    for block, array, at in shards_of(here[0], pieces):
+    return lax.rsqrt(square * (1.0 / 4096) + EPSILON)
+
+
+def project(layer, x, gain, inv_scale, found, turned):
+    for block, array, at in found:
         t = 2 * block
         left = (x[t].astype(F32) * inv_scale * gain[layer, pl.ds(t, 1), :]).astype(BF16)
         right = (x[t + 1].astype(F32) * inv_scale * gain[layer, pl.ds(t + 1, 1), :]).astype(BF16)
         rows = jnp.concatenate([left, right], axis=1)
         turned += lax.dot_general(array[at, :, 128 * layer : 128 * layer + 256], rows, (((1,), (1,)), ((), ())), preferred_element_type=F32)
+    return turned
+
+
+def half_kernel(here, x, gain, drive_far, read_far, joined, scale, partial, drive, read, sems):
+    copies = [pltpu.make_async_copy(a.at[0], b, sems.at[i]) for i, (a, b) in enumerate(((drive_far, drive), (read_far, read)))]
+    for copy in copies:
+        copy.start()
+    inv_scale = scale_of(x)
+    scale[...] = jnp.broadcast_to(inv_scale, scale.shape)
+    partial[...] = project(0, x, gain, inv_scale, shards_of(here[0], [joined, joined])[:8], jnp.zeros((128, 16), F32))
+    for copy in copies:
+        copy.wait()
+
+
+def rest_kernel(here, x, gain, decay, skip, old, across, scale, partial, drive, read, mixed, fresh_out):
+    turned = project(0, x, gain, scale[...], shards_of(here[0], [across, across])[8:], partial[...])
+    finish(0, turned, drive, read, decay, skip, old, mixed, fresh_out)
+
+
+def mixer_kernel(here, x, gain, drive_far, read_far, decay, skip, old, joined, across, mixed, fresh_out, drive, read, sems):
+    copies = [pltpu.make_async_copy(a.at[1], b, sems.at[i]) for i, (a, b) in enumerate(((drive_far, drive), (read_far, read)))]
+    for copy in copies:
+        copy.start()
+    turned = project(1, x, gain, scale_of(x), shards_of(here[0], [joined, across]), jnp.zeros((128, 16), F32))
+    for copy in copies:
+        copy.wait()
+    finish(1, turned, drive, read, decay, skip, old, mixed, fresh_out)
+
+
+def finish(layer, turned, drive, read, decay, skip, old, mixed, fresh_out):
     both = turned.T.astype(BF16).astype(F32)
-    get_drive.wait()
     parts = jnp.dot(both.astype(BF16), drive[...], preferred_element_type=F32)
     push = parts[:, :512] + parts[:, 512:]
     d_re, d_im = decay[layer, 0:1], decay[layer, 1:2]
@@ -150,7 +176,6 @@
     f_im = d_re * o_im + d_im * o_re + push[:, 256:]
     fresh = jnp.concatenate([f_re, f_im], axis=1)
     fresh_out[...] = fresh
-    get_read.wait()
     upper, lower = halves(fresh)
     contract = (((1,), (1,)), ((), ()))
     parts = lax.dot_general(jnp.concatenate([upper, lower]), read[:, :512], contract, preferred_element_type=F32)
@@ -217,22 +242,22 @@
     )(*args)
 
 
-def mixer_call(layer, here, x, small, pieces):
-    gain, drive, read, decay, skip, old = small
-    args = [here, *close(x, gain), drive, read, *close(decay, skip, old, *pieces)]
+def far_call(kernel, args, far, shapes, near, scratch=()):
     specs = [SMEM] + [VMEM] * (len(args) - 1)
-    for at in (3, 4):
+    for at in far:
         args[at] = pltpu.with_memory_space_constraint(args[at], pltpu.HBM)
         specs[at] = pl.BlockSpec(memory_space=pltpu.HBM)
     return pl.pallas_call(
-        functools.partial(mixer_kernel, layer),
+        kernel,
         in_specs=specs,
-        out_specs=[VMEM] * 2,
-        out_shape=[jax.ShapeDtypeStruct((32, 8, 128), BF16), pltpu.VMEM((16, 512), F32)],
-        scratch_shapes=[pltpu.VMEM((128, 1024), BF16)] * 2 + [pltpu.SemaphoreType.DMA((2,))],
+        out_specs=[VMEM] * len(shapes),
+        out_shape=[pltpu.VMEM(*s) if i in near else jax.ShapeDtypeStruct(*s) for i, s in enumerate(shapes)],
+        scratch_shapes=[*scratch, pltpu.SemaphoreType.DMA((2,))],
         compiler_params=pltpu.CompilerParams(vmem_limit_bytes=16 << 20),
-        name="mixer_step",
     )(*args)
+
+
+MIXED = [((32, 8, 128), BF16), ((16, 512), F32)]
 
 
 def local(tokens, norm_gain, w_in, w_gate, decay_rate, frequency, log_step, map_re, map_im, read_re, read_im, skip_weight, w_out, state_re, state_im):
@@ -261,13 +286,19 @@
 
     gathered = over_tp(copies)
     first = pieces_of(both0)
-    mixed, fresh0 = mixer_call(0, here, gathered, small, first)
+    gain, drive, read, decay, skip, old = small
+    shapes = [((16, 128), F32), ((128, 16), F32), ((128, 1024), BF16), ((128, 1024), BF16)]
+    args = [here, *close(gathered, gain), drive, read, *close(first[0])]
+    halfway = far_call(half_kernel, args, (3, 4), shapes, range(4))
+    args = (here, *close(gathered, gain, decay, skip, old, first[1], *halfway))
+    mixed, fresh0 = run(rest_kernel, args, MIXED, (1,), 1)
     second = pieces_of(both1)
     mixed = over_tp(mixed)
     shapes = [((16, 128), BF16), ((32, 16, 128), BF16)]
     hidden, copies = run(functools.partial(out_kernel, 0), (here, *close(mixed), tokens, *close(*second)), shapes, (0,), 1)
     gathered = over_tp(copies)
-    mixed, fresh1 = mixer_call(1, here, gathered, small, second)
+    args = [here, *close(gathered, gain), drive, read, *close(decay, skip, old, *second)]
+    mixed, fresh1 = far_call(mixer_kernel, args, (3, 4), MIXED, (1,), [pltpu.VMEM((128, 1024), BF16)] * 2)
     shapes = [((16, 128), BF16), (state_re.shape, F32), (state_im.shape, F32)]
     args = (here, *close(over_tp(mixed), hidden, *second, fresh0, fresh1))
     return tuple(run(functools.partial(out_kernel, 1), args, shapes, (), 1))

time: 125 us -> 126 us (level)
  no operation moved by 1% of the time
where the time goes in v4:
time: 126 us; the launch traced here: 125 us
  waiting for transfers between devices  45.3 us (36%)
  blocking collectives  40.3 us (32%)
  starting transfers between devices  28.8 us (23%)
  Pallas kernels  9.91 us (8%)
    all_to_all x3, blocking collectives, over_tp(): return lax.all_to_all(copies, 'tp', split_axis=0, concat_axis=0, tiled=True)  40.3 us
    ppermute x3, waiting for transfers between devices, from_y(): return lax.ppermute(array, 'dp', pairs)  32.7 us
    all_to_all x1, starting transfers between devices, over_tp(): return lax.all_to_all(copies, 'tp', split_axis=0, concat_axis=0, tiled=True)  12.8 us
    all_to_all x1, waiting for transfers between devices, over_tp(): return lax.all_to_all(copies, 'tp', split_axis=0, concat_axis=0, tiled=True)  8.56 us
    ppermute x3, starting transfers between devices, from_y(): return lax.ppermute(array, 'dp', pairs)  7.96 us
    pallas_call x3, Pallas kernels, run_loaded(): pl.pallas_call(loaded(kernel, len(args), len(shapes)), in_specs=[pl.Block...  4.8 us
    ppermute x1, starting transfers between devices, local(): pair = jnp.concatenate([shard, lax.ppermute(shard, 'dp', DIAGONAL)])  4.13 us
    ppermute x1, waiting for transfers between devices, local(): pair = jnp.concatenate([shard, lax.ppermute(shard, 'dp', DIAGONAL)])  4.06 us
  transfers between devices with their start and end apart: 7, of which 5 were waited for; matrix products, arithmetic and copies ran while one was open for 0% of the time, Pallas kernels for 5%

profile of v4, /device:TPU:24, one launch (start us, length us, event | category | flops | bytes accessed | tf_op | source)
XLA Modules:
  0.0 125.1 jit_solution(15958114404999329623)
XLA Ops:
  0.6 0.9 shard_map.168
  1.6 4.1 %collective-permute-start = (bf16[1,128,768]{2,1,0:T(8,128)(2,1)S(1)}, bf16[1,128,768]{2,1,0:T(8,128)(2,1)S(1)}, u32[]{:S(2)}, u32[]{:S(2)}) collective-permute-start(bf16[1,128,768]{2,1,0:T(8,128)(2,1)S(1)} %shard_map.168), channel_id=1, source_target_pairs={{3,0},{5,2},{7,4},{9,6},{11,8},{13,10},{15,12},{1,14},{14,1},{0,3}... | collective-permute-start | bytes 589832 | tf_op jit(solution)/shard_map/ppermute | solution.py:277
  5.7 4.1 %collective-permute-done = bf16[1,128,768]{2,1,0:T(8,128)(2,1)S(1)} collective-permute-done((bf16[1,128,768]{2,1,0:T(8,128)(2,1)S(1)}, bf16[1,128,768]{2,1,0:T(8,128)(2,1)S(1)}, u32[]{:S(2)}, u32[]{:S(2)}) %collective-permute-start) | collective-permute-done | bytes 196640 | tf_op jit(solution)/shard_map/ppermute | solution.py:277
  9.8 1.9 %collective-permute-start.1 = (bf16[2,128,768]{2,1,0:T(8,128)(2,1)S(1)}, bf16[2,128,768]{2,1,0:T(8,128)(2,1)S(1)}, u32[]{:S(2)}, u32[]{:S(2)}) collective-permute-start(bf16[2,128,768]{2,1,0:T(8,128)(2,1)S(1)} %pad_maximum_fusion.pair), channel_id=1, source_target_pairs={{2,0},{4,2},{6,4},{8,6},{10,8},{12,10},{14,12},{0,14},{15,1},{1,3}... | collective-permute-start | bytes 1179656 | tf_op jit(solution)/shard_map/ppermute | solution.py:26
  11.8 9.0 %collective-permute-done.1.near = bf16[2,128,768]{2,1,0:T(8,128)(2,1)S(1)} collective-permute-done((bf16[2,128,768]{2,1,0:T(8,128)(2,1)S(1)}, bf16[2,128,768]{2,1,0:T(8,128)(2,1)S(1)}, u32[]{:S(2)}, u32[]{:S(2)}) %collective-permute-start.1) | collective-permute-done | bytes 393248 | tf_op jit(solution)/shard_map/ppermute | solution.py:26
  20.7 0.1 shard_map.169
  20.8 3.1 %collective-permute-start.4 = (bf16[4,128,512]{2,1,0:T(8,128)(2,1)S(1)}, bf16[4,128,512]{2,1,0:T(8,128)(2,1)S(1)}, u32[]{:S(2)}, u32[]{:S(2)}) collective-permute-start(bf16[4,128,512]{2,1,0:T(8,128)(2,1)S(1)} %get-tuple-element.33.both), channel_id=1, source_target_pairs={{4,0},{6,2},{8,4},{10,6},{12,8},{14,10},{0,12},{2,14},{13,1},{15,3... | collective-permute-start | bytes 1572872 | tf_op jit(solution)/shard_map/ppermute | solution.py:26
  23.9 14.5 %collective-permute-done.4.far = bf16[4,128,512]{2,1,0:T(8,128)(2,1)S(1)} collective-permute-done((bf16[4,128,512]{2,1,0:T(8,128)(2,1)S(1)}, bf16[4,128,512]{2,1,0:T(8,128)(2,1)S(1)}, u32[]{:S(2)}, u32[]{:S(2)}) %collective-permute-start.4) | collective-permute-done | bytes 524320 | tf_op jit(solution)/shard_map/ppermute | solution.py:26
  38.4 0.1 shard_map.173.rest_0_.joined
  38.5 1.9 %collective-permute-start.5 = (bf16[8,128,512]{2,1,0:T(8,128)(2,1)S(1)}, bf16[8,128,512]{2,1,0:T(8,128)(2,1)S(1)}, u32[]{:S(2)}, u32[]{:S(2)}) collective-permute-start(bf16[8,128,512]{2,1,0:T(8,128)(2,1)S(1)} %shard_map.173.rest_0_.joined), channel_id=1, source_target_pairs={{0,1},{1,0},{2,3},{3,2},{4,5},{5,4},{6,7},{7,6},{8,9},{9,8},{10,11... | collective-permute-start | bytes 3145736 | tf_op jit(solution)/shard_map/ppermute | solution.py:21
  40.4 2.9 %collective-permute-start.2 = (bf16[4,128,256]{2,1,0:T(8,128)(2,1)S(1)}, bf16[4,128,256]{2,1,0:T(8,128)(2,1)S(1)}, u32[]{:S(2)}, u32[]{:S(2)}) collective-permute-start(bf16[4,128,256]{2,1,0:T(8,128)(2,1)S(1)} %get-tuple-element.25.both), channel_id=1, source_target_pairs={{4,0},{6,2},{8,4},{10,6},{12,8},{14,10},{0,12},{2,14},{13,1},{15,3... | collective-permute-start | bytes 786440 | tf_op jit(solution)/shard_map/ppermute | solution.py:26
  43.3 9.3 %collective-permute-done.2.far = bf16[4,128,256]{2,1,0:T(8,128)(2,1)S(1)} collective-permute-done((bf16[4,128,256]{2,1,0:T(8,128)(2,1)S(1)}, bf16[4,128,256]{2,1,0:T(8,128)(2,1)S(1)}, u32[]{:S(2)}, u32[]{:S(2)}) %collective-permute-start.2) | collective-permute-done | bytes 262176 | tf_op jit(solution)/shard_map/ppermute | solution.py:26
  52.6 1.9 %collective-permute-start.3 = (bf16[8,128,256]{2,1,0:T(8,128)(2,1)S(1)}, bf16[8,128,256]{2,1,0:T(8,128)(2,1)S(1)}, u32[]{:S(2)}, u32[]{:S(2)}) collective-permute-start(bf16[8,128,256]{2,1,0:T(8,128)(2,1)S(1)} %shard_map.170.joined), channel_id=1, source_target_pairs={{0,1},{1,0},{2,3},{3,2},{4,5},{5,4},{6,7},{7,6},{8,9},{9,8},{10,11... | collective-permute-start | bytes 1572872 | tf_op jit(solution)/shard_map/ppermute | solution.py:21
  54.6 1.4 %shard_map.166 = bf16[32,16,128]{2,1,0:T(8,128)(2,1)} custom-call(bf16[16,128]{1,0:T(8,128)(2,1)} %before.1), custom_call_target="tpu_custom_call" | custom-call | tf_op jit(solution)/shard_map/pallas_call | solution.py:235
  55.9 12.8 %all-to-all-start = ((bf16[32,16,128]{2,1,0:T(8,128)(2,1)}), bf16[32,16,128]{2,1,0:T(8,128)(2,1)S(1)}, u32[]{:S(2)}, u32[]{:S(2)}) async-start(bf16[32,16,128]{2,1,0:T(8,128)(2,1)} %shard_map.166), calls=%async_computation | async-start | bytes 262144 | tf_op jit(solution)/shard_map/all_to_all | solution.py:40
  68.8 2.5 %shard_map.167 = (f32[2,32,128]{2,1,0:T(8,128)S(1)}, bf16[2,128,1024]{2,1,0:T(8,128)(2,1)}, bf16[2,128,1024]{2,1,0:T(8,128)(2,1)}, f32[2,2,256]{2,1,0:T(2,128)S(...) custom-call(f32[2,4096]{1,0:T(2,128)} %refs_0_.3, f32[2,4,64]{2,1,0:T(4,128)} %refs_1_.1, ...), custom_call_target="tpu_custom_call" | custom-call | tf_op jit(solution)/shard_map/pallas_call | solution.py:235
  71.3 8.6 %all-to-all-done.x = bf16[32,16,128]{2,1,0:T(8,128)(2,1)S(1)} async-done(((bf16[32,16,128]{2,1,0:T(8,128)(2,1)}), bf16[32,16,128]{2,1,0:T(8,128)(2,1)S(1)}, u32[]{:S(2)}, u32[]{:S(2)}) %all-to-all-start) | async-done | bytes 131104 | tf_op jit(solution)/shard_map/all_to_all | solution.py:40
  79.8 1.2 shard_map.171
  81.0 0.0 collective-permute-done.3.across
  81.0 0.9 shard_map.172
  81.9 0.0 copy-start
  81.9 13.5 %all_to_all.20.mixed = bf16[32,8,128]{2,1,0:T(8,128)(2,1)S(1)} all-to-all(bf16[32,8,128]{2,1,0:T(8,128)(2,1)S(1)} %get-tuple-element.32), channel_id=1, replica_groups=mesh['tp'=32,'dp'=16] {'tp'}, dimensions={0} | all-to-all | bytes 131072 | tf_op jit(solution)/shard_map/all_to_all | solution.py:40
  95.4 0.0 collective-permute-done.5.rest_1_.across
  95.4 0.0 copy-done
  95.4 0.3 shard_map.174
  95.7 13.7 %all_to_all.21.x = bf16[32,16,128]{2,1,0:T(8,128)(2,1)S(1)} all-to-all(bf16[32,16,128]{2,1,0:T(8,128)(2,1)S(1)} %get-tuple-element.34), channel_id=1, replica_groups=mesh['tp'=32,'dp'=16] {'tp'}, dimensions={0} | all-to-all | bytes 262144 | tf_op jit(solution)/shard_map/all_to_all | solution.py:40
  109.4 1.7 %shard_map.175 = (bf16[32,8,128]{2,1,0:T(8,128)(2,1)S(1)}, f32[16,512]{1,0:T(8,128)S(1)}) custom-call(s32[1]{0:T(128)} %bitcast.here, bf16[32,16,128]{2,1,0:T(8,128)(2,1)S(1)} %all_to_all.21.x, f32[2,32,128]{2,1,0:T(8,128)S(1)} %get-tuple-element.21.gain, bf16[2,128,1024]{2,1,0:T(8,128)(2,1)} %get-tuple-element.26.drive_far, ...), custom_call_target="tpu_custom_call" | custom-call | tf_op jit(solution)/shard_map/pallas_call | solution.py:250
  111.1 13.1 %all_to_all.22.mixed = bf16[32,8,128]{2,1,0:T(8,128)(2,1)S(1)} all-to-all(bf16[32,8,128]{2,1,0:T(8,128)(2,1)S(1)} %get-tuple-element.35), channel_id=1, replica_groups=mesh['tp'=32,'dp'=16] {'tp'}, dimensions={0} | all-to-all | bytes 131072 | tf_op jit(solution)/shard_map/all_to_all | solution.py:40
  124.2 0.9 shard_map.176
  (2 shorter events, 0.1 us)
Async XLA Ops:
  1.6 8.2 %collective-permute-start = (bf16[1,128,768]{2,1,0:T(8,128)(2,1)S(1)}, bf16[1,128,768]{2,1,0:T(8,128)(2,1)S(1)}, u32[]{:S(2)}, u32[]{:S(2)}) collective-permute-start(bf16[1,128,768]{2,1,0:T(8,128)(2,1)S(1)} %shard_map.168), channel_id=1, source_target_pairs={{3,0},{5,2},{7,4},{9,6},{11,8},{13,10},{15,12},{1,14},{14,1},{0,3}... | collective-permute-start | bytes 589832 | tf_op jit(solution)/shard_map/ppermute | solution.py:277
  9.8 10.9 %collective-permute-start.1 = (bf16[2,128,768]{2,1,0:T(8,128)(2,1)S(1)}, bf16[2,128,768]{2,1,0:T(8,128)(2,1)S(1)}, u32[]{:S(2)}, u32[]{:S(2)}) collective-permute-start(bf16[2,128,768]{2,1,0:T(8,128)(2,1)S(1)} %pad_maximum_fusion.pair), channel_id=1, source_target_pairs={{2,0},{4,2},{6,4},{8,6},{10,8},{12,10},{14,12},{0,14},{15,1},{1,3}... | collective-permute-start | bytes 1179656 | tf_op jit(solution)/shard_map/ppermute | solution.py:26
  20.8 17.7 %collective-permute-start.4 = (bf16[4,128,512]{2,1,0:T(8,128)(2,1)S(1)}, bf16[4,128,512]{2,1,0:T(8,128)(2,1)S(1)}, u32[]{:S(2)}, u32[]{:S(2)}) collective-permute-start(bf16[4,128,512]{2,1,0:T(8,128)(2,1)S(1)} %get-tuple-element.33.both), channel_id=1, source_target_pairs={{4,0},{6,2},{8,4},{10,6},{12,8},{14,10},{0,12},{2,14},{13,1},{15,3... | collective-permute-start | bytes 1572872 | tf_op jit(solution)/shard_map/ppermute | solution.py:26
  38.5 56.9 %collective-permute-start.5 = (bf16[8,128,512]{2,1,0:T(8,128)(2,1)S(1)}, bf16[8,128,512]{2,1,0:T(8,128)(2,1)S(1)}, u32[]{:S(2)}, u32[]{:S(2)}) collective-permute-start(bf16[8,128,512]{2,1,0:T(8,128)(2,1)S(1)} %shard_map.173.rest_0_.joined), channel_id=1, source_target_pairs={{0,1},{1,0},{2,3},{3,2},{4,5},{5,4},{6,7},{7,6},{8,9},{9,8},{10,11... | collective-permute-start | bytes 3145736 | tf_op jit(solution)/shard_map/ppermute | solution.py:21
  40.4 12.2 %collective-permute-start.2 = (bf16[4,128,256]{2,1,0:T(8,128)(2,1)S(1)}, bf16[4,128,256]{2,1,0:T(8,128)(2,1)S(1)}, u32[]{:S(2)}, u32[]{:S(2)}) collective-permute-start(bf16[4,128,256]{2,1,0:T(8,128)(2,1)S(1)} %get-tuple-element.25.both), channel_id=1, source_target_pairs={{4,0},{6,2},{8,4},{10,6},{12,8},{14,10},{0,12},{2,14},{13,1},{15,3... | collective-permute-start | bytes 786440 | tf_op jit(solution)/shard_map/ppermute | solution.py:26
  52.6 28.4 %collective-permute-start.3 = (bf16[8,128,256]{2,1,0:T(8,128)(2,1)S(1)}, bf16[8,128,256]{2,1,0:T(8,128)(2,1)S(1)}, u32[]{:S(2)}, u32[]{:S(2)}) collective-permute-start(bf16[8,128,256]{2,1,0:T(8,128)(2,1)S(1)} %shard_map.170.joined), channel_id=1, source_target_pairs={{0,1},{1,0},{2,3},{3,2},{4,5},{5,4},{6,7},{7,6},{8,9},{9,8},{10,11... | collective-permute-start | bytes 1572872 | tf_op jit(solution)/shard_map/ppermute | solution.py:21
  55.9 23.9 %all-to-all-start = ((bf16[32,16,128]{2,1,0:T(8,128)(2,1)}), bf16[32,16,128]{2,1,0:T(8,128)(2,1)S(1)}, u32[]{:S(2)}, u32[]{:S(2)}) async-start(bf16[32,16,128]{2,1,0:T(8,128)(2,1)} %shard_map.166), calls=%async_computation | async-start | bytes 262144 | tf_op jit(solution)/shard_map/all_to_all | solution.py:40
  81.9 13.5 %copy-start = (bf16[16,128]{1,0:T(8,128)(2,1)S(1)}, bf16[16,128]{1,0:T(8,128)(2,1)}, u32[]{:S(2)}) copy-start(bf16[16,128]{1,0:T(8,128)(2,1)} %before.1) | copy-start | bytes 12292
